TPU v7x, 512 devices: a whole 4x4x16 slice. The times are simulated.
512 devices in a mesh: sp: 64 (over z, y), tp: 8 (over x, core).
Axes of the slice: x: 4, y: 4, z: 16, core: 2. Of those that a mesh axis runs over, the one named last changes fastest.
Arguments:
- queries: bfloat16 [12288, 1024], P('sp', 'tp'), may hold values from -6 to 6
- keys: bfloat16 [12288, 512], P('sp', 'tp'), may hold values from -6 to 6
- values: bfloat16 [12288, 512], P('sp', 'tp'), may hold values from -6 to 6
- query_gain: float32 [16, 64], P('tp'), may hold values from 1.4 to 7.5
- key_gain: float32 [8, 64], P('tp'), may hold values from 1.4 to 7.5
- out_weight: bfloat16 [1024, 2048], P('tp'), may hold values from -0.375 to 0.375
- residual: bfloat16 [12288, 2048], P('sp'), may hold values from -170 to 170
- norm_gain: float32 [2048], replicated, may hold values from 0.1 to 1.9
- gate_weight: bfloat16 [2048, 5632], P('sp', 'tp'), may hold values from -0.125 to 0.125
- up_weight: bfloat16 [2048, 5632], P('sp', 'tp'), may hold values from -0.125 to 0.125
- down_weight: bfloat16 [5632, 2048], P('tp', 'sp'), may hold values from -0.15625 to 0.15625
Outputs:
- mixed: bfloat16 [12288, 2048], P('sp')
All inputs are finite; a program needn't handle non-finite values.
Results may differ from a plain program's by a relative error of at most 0.017.
Values may be sent and summed in bfloat16 or wider, within the bound.
A program may use at most 64 MiB of HBM per device.

v0:
```python
import jax
import jax.numpy as jnp
from jax import lax
from jax.sharding import PartitionSpec as P

GRID_W = 64


epsilon = 1e-06
rope_base = 10000.0
block_keys = 2048


def turned_gather(arrays, axis, dims):
    turned = [jnp.moveaxis(a, dim, 0) for a, dim in zip(arrays, dims)]
    both = jnp.concatenate([t.reshape(len(t), -1) for t in turned], axis=1)
    filled, at, gathered = (lax.all_gather(both, axis, axis=0, tiled=True), 0, [])
    for t, dim in zip(turned, dims):
        slab = filled[:, at : at + t[0].size].reshape(-1, *t.shape[1:])
        gathered.append(jnp.moveaxis(slab, 0, dim))
        at += t[0].size
    return tuple(gathered)


def in_one_piece(arrays, axis, dim, along):
    ends, at = ([], 0)
    for a in arrays[:-1]:
        at += a.shape[along]
        ends.append(at)
    both = jnp.concatenate(arrays, axis=along)
    return tuple(jnp.split(lax.all_gather(both, axis, axis=dim, tiled=True), ends, axis=along))


def split_up(array, dim, peers):
    dims = array.shape
    parts = array.reshape(*dims[:dim], peers, dims[dim] // peers, *dims[dim + 1 :])
    return jnp.moveaxis(parts, dim, 0)


def summed_on_arrival(array, axis, dim):
    parts = split_up(array, dim, lax.axis_size(axis))
    arrived = lax.all_to_all(parts, axis, split_axis=0, concat_axis=0, tiled=True)
    return arrived.astype(jnp.float32).sum(axis=0)


def laid_out(parts, dim):
    dims = list(parts.shape[1:])
    dims[dim] *= parts.shape[0]
    return jnp.moveaxis(parts, 0, dim).reshape(dims)


def copy_for_each(array, axis):
    peers = lax.axis_size(axis)
    return lax.all_to_all(
        jnp.broadcast_to(array[None], (peers, *array.shape)), axis, 0, 0, tiled=True
    )


def collect(array, axis, dim):
    return laid_out(copy_for_each(array, axis), dim)


def rotate_pairs(entries, places):
    half = entries.shape[-1] // 2
    frequency = rope_base ** (-jnp.arange(half, dtype=jnp.float32) / half)
    angle = places.astype(jnp.float32)[:, None, None] * frequency[None, None, :]
    cosine = jnp.cos(angle)
    sine = jnp.sin(angle)
    first = entries[..., :half]
    second = entries[..., half:]
    return jnp.concatenate(
        [first * cosine - second * sine, first * sine + second * cosine], axis=-1
    )


def grid_rotate(entries, grid_rows, grid_cols):
    half = entries.shape[-1] // 2
    return jnp.concatenate(
        [
            rotate_pairs(entries[..., :half], grid_rows),
            rotate_pairs(entries[..., half:], grid_cols),
        ],
        axis=-1,
    )


def head_norm(entries, gains):
    factor = lax.rsqrt(jnp.mean(entries * entries, axis=-1, keepdims=True) + epsilon)
    return entries * factor * gains[None]


def row_norm(mid, norm_gain):
    wide = mid.astype(jnp.float32)
    return (
        wide * lax.rsqrt(jnp.mean(wide * wide, axis=-1, keepdims=True) + epsilon) * norm_gain
    ).astype(jnp.bfloat16)


def block_span(length):
    span = block_keys
    while length % span != 0:
        span = span - 1
    return span


def body(
    queries,
    keys,
    values,
    query_gain,
    key_gain,
    out_weight,
    residual,
    norm_gain,
    gate_weight,
    up_weight,
    down_weight,
):
    own = queries.shape[0]
    heads = query_gain.shape[0]
    key_heads = key_gain.shape[0]
    head_size = query_gain.shape[1]
    group = heads // key_heads
    gate_full, up_full, down_full = turned_gather(
        (gate_weight, up_weight, down_weight), "sp", (0, 0, 1)
    )
    places = lax.axis_index("sp") * own + jnp.arange(own, dtype=jnp.int32)
    grid_rows = places // GRID_W
    grid_cols = places % GRID_W
    query_turned = grid_rotate(
        head_norm(queries.astype(jnp.float32).reshape(own, heads, head_size), query_gain),
        grid_rows,
        grid_cols,
    ).astype(jnp.bfloat16)
    query_groups = query_turned.reshape(own, key_heads, group, head_size)
    key_turned = (
        grid_rotate(
            head_norm(keys.astype(jnp.float32).reshape(own, key_heads, head_size), key_gain),
            grid_rows,
            grid_cols,
        )
        .astype(jnp.bfloat16)
        .reshape(own, key_heads * head_size)
    )
    scale = head_size ** (-0.5)

    def absorb(carry, key_block, value_block):
        top, total, summed = carry
        key_block = key_block.reshape(-1, key_heads, head_size)
        value_block = value_block.reshape(-1, key_heads, head_size)
        score = (
            jnp.einsum(
                "qgrd,kgd->qgrk", query_groups, key_block, preferred_element_type=jnp.float32
            )
            * scale
        )
        new_top = jnp.maximum(top, jnp.max(score, axis=-1))
        weight = jnp.exp(score - new_top[..., None])
        shrink = jnp.exp(top - new_top)
        total = total * shrink + jnp.sum(weight, axis=-1)
        summed = summed * shrink[..., None] + jnp.einsum(
            "qgrk,kgd->qgrd",
            weight.astype(jnp.bfloat16),
            value_block,
            preferred_element_type=jnp.float32,
        )
        return (new_top, total, summed)

    start_state = (
        jnp.full((own, key_heads, group), -jnp.inf, jnp.float32),
        jnp.zeros((own, key_heads, group), jnp.float32),
        jnp.zeros((own, key_heads, group, head_size), jnp.float32),
    )
    pieces = in_one_piece((key_turned, values), "sp", 0, 1)
    length = pieces[0].shape[0]
    span = block_span(length)
    width = pieces[0].shape[1]
    key_blocks = pieces[0].reshape(length // span, span, width)
    value_blocks = pieces[1].reshape(length // span, span, width)

    def scan_step(inner, blocks):
        return (absorb(inner, blocks[0], blocks[1]), None)

    result, unused = lax.scan(scan_step, start_state, (key_blocks, value_blocks))
    top, total, summed = result
    attended = (summed / total[..., None]).reshape(own, heads * head_size).astype(jnp.bfloat16)
    part_rows = own // lax.axis_size("tp")
    branch = summed_on_arrival(
        jnp.dot(attended, out_weight, preferred_element_type=jnp.float32).astype(jnp.bfloat16),
        "tp",
        0,
    )
    own_rows = lax.dynamic_slice_in_dim(residual, lax.axis_index("tp") * part_rows, part_rows, 0)
    mid = (own_rows.astype(jnp.float32) + branch).astype(jnp.bfloat16)
    normed_all = collect(row_norm(mid, norm_gain), "tp", 0)
    gate = jnp.dot(normed_all, gate_full, preferred_element_type=jnp.float32)
    up_value = jnp.dot(normed_all, up_full, preferred_element_type=jnp.float32)
    hidden = (jax.nn.silu(gate) * up_value).astype(jnp.bfloat16)
    terms = jnp.dot(hidden, down_full, preferred_element_type=jnp.float32)
    ffn = summed_on_arrival(terms.astype(jnp.bfloat16), "tp", 0)
    finished = (mid.astype(jnp.float32) + ffn).astype(jnp.bfloat16)
    return collect(finished, "tp", 0)


def solution(mesh):
    in_specs = (
        P("sp", "tp"),
        P("sp", "tp"),
        P("sp", "tp"),
        P("tp", None),
        P("tp", None),
        P("tp", None),
        P("sp", None),
        P(),
        P("sp", "tp"),
        P("sp", "tp"),
        P("tp", "sp"),
    )
    out_specs = P("sp", None)
    return jax.shard_map(body, mesh=mesh, in_specs=in_specs, out_specs=out_specs, check_vma=False)
```

profile of v0, /device:TPU:1, one launch (start us, length us, event | category | flops | bytes accessed | tf_op | source)
XLA Modules:
  0.0 363.2 jit_solution(17226902989139248117)
XLA Ops:
  7.4 0.8 fusion.50
  8.9 0.9 copy.27
  10.7 1.6 concatenate.49
  12.3 0.9 copy.29
  14.3 136.2 %all-gather.3.cloned.1.call-done = bf16[12288,128]{1,0:T(8,128)(2,1)} async-done(((bf16[192,128]{1,0:T(8,128)(2,1)}), bf16[12288,128]{1,0:T(8,128)(2,1)}) %all-gather.3.cloned.1.call-update) | async-done | bytes 3145744 | tf_op jit(solution)/shard_map/all_gather | solution.py:31
  150.5 6.2 %fusion.79 = (bf16[12288,64]{1,0:T(8,128)(2,1)}, bf16[12288,64]{1,0:T(8,128)(2,1)}) fusion(bf16[12288,128]{1,0:T(8,128)(2,1)} %all-gather.3.cloned.1.call-done), kind=kLoop, calls=%fused_computation.111 | loop fusion | bytes 6291456 | tf_op jit(solution)/shard_map/split | solution.py:31
  156.7 3.1 copy.31
  159.8 4.3 %copy.32 = bf16[6,2048,64]{1,2,0:T(8,128)(2,1)} copy(bf16[6,2048,64]{2,1,0:T(8,128)(2,1)} %bitcast.111) | data formatting | bytes 3145728
  164.1 35.0 %while.15 = (s32[]{:T(128)}, f32[192,1,2]{0,2,1:T(2,128)S(1)}, f32[192,1,2]{0,2,1:T(2,128)S(1)}, f32[192,1,2,64]{0,3,2,1:T(8,128)S(1)}, bf16[6,2048,64]{1,2,0:T(...) while((s32[]{:T(128)}, f32[192,1,2]{0,2,1:T(2,128)S(1)}, ...), condition=%wide.region_5.6_spmd.clone, body=%wide.region_2.5_spmd.clone.sunk | while | flops 206121216 | bytes 22831752 | solution.py:184
  164.1 2.3 bitcast_reduce_fusion.2
  166.4 2.8 fusion.93
  169.9 2.3 bitcast_reduce_fusion.2
  172.2 2.8 fusion.93
  175.8 2.3 bitcast_reduce_fusion.2
  178.1 2.8 fusion.93
  181.6 2.3 bitcast_reduce_fusion.2
  183.9 2.8 fusion.93
  187.4 2.3 bitcast_reduce_fusion.2
  189.7 2.8 fusion.93
  193.3 2.3 bitcast_reduce_fusion.2
  195.6 2.8 fusion.93
  199.1 1.3 convolution_convert_fusion
  200.4 13.7 %all-to-all-start = ((bf16[8,24,2048]{2,1,0:T(8,128)(2,1)}), bf16[8,24,2048]{2,1,0:T(8,128)(2,1)S(1)}, u32[]{:S(2)}, u32[]{:S(2)}) async-start(bf16[8,24,2048]{2,1,0:T(8,128)(2,1)} %bitcast.15), calls=%async_computation | async-start | bytes 1572864 | tf_op jit(solution)/shard_map/all_to_all | solution.py:42
  214.0 12.2 %all-to-all-done = bf16[8,24,2048]{2,1,0:T(8,128)(2,1)S(1)} async-done(((bf16[8,24,2048]{2,1,0:T(8,128)(2,1)}), bf16[8,24,2048]{2,1,0:T(8,128)(2,1)S(1)}, u32[]{:S(2)}, u32[]{:S(2)}) %all-to-all-start) | async-done | bytes 786464 | tf_op jit(solution)/shard_map/all_to_all | solution.py:42
  226.3 1.0 fusion.44
  227.5 15.5 %all_to_all.20 = bf16[8,24,2048]{2,1,0:T(8,128)(2,1)S(1)} all-to-all(bf16[8,24,2048]{2,1,0:T(8,128)(2,1)S(1)} %broadcast_in_dim.13), channel_id=1, replica_groups=mesh['sp'=64,'tp'=8] {'tp'}, dimensions={0} | all-to-all | bytes 1572864 | tf_op jit(solution)/shard_map/all_to_all | solution.py:54
  243.1 64.2 %all-gather.5.cloned.1.call-done = bf16[2048,2112]{1,0:T(8,128)(2,1)} async-done(((bf16[32,2112]{1,0:T(8,128)(2,1)}), bf16[2048,2112]{1,0:T(8,128)(2,1)}) %all-gather.5.cloned.1.call-update) | async-done | bytes 8650768 | tf_op jit(solution)/shard_map/all_gather | solution.py:17
  307.3 2.7 fusion.25
  309.9 5.2 %fusion.27 = bf16[192,2048]{1,0:T(8,128)(2,1)S(1)} fusion(bf16[2048,2112]{1,0:T(8,128)(2,1)} %all-gather.5.cloned.1.call-done, bf16[192,2048]{1,0:T(8,128)(2,1)S(1)} %bitcast.117, f32[192,704]{1,0:T(8,128)S(1)} %fusion.25), kind=kOutput, calls=%fused_computation.31 | convolution fusion | flops 1108500480 | bytes 8404992 | tf_op jit(solution)/shard_map/dot_general | solution.py:199
  315.2 24.5 %all_to_all.21 = bf16[8,24,2048]{2,1,0:T(8,128)(2,1)S(1)} all-to-all(bf16[8,24,2048]{2,1,0:T(8,128)(2,1)S(1)} %bitcast.118), channel_id=1, replica_groups=mesh['sp'=64,'tp'=8] {'tp'}, dimensions={0} | all-to-all | bytes 1572864 | tf_op jit(solution)/shard_map/all_to_all | solution.py:42
  339.9 15.6 %all_to_all.22 = bf16[8,24,2048]{2,1,0:T(8,128)(2,1)S(1)} all-to-all(bf16[8,24,2048]{2,1,0:T(8,128)(2,1)S(1)} %broadcast_in_dim.14), channel_id=1, replica_groups=mesh['sp'=64,'tp'=8] {'tp'}, dimensions={0} | all-to-all | bytes 1572864 | tf_op jit(solution)/shard_map/all_to_all | solution.py:54
  355.4 0.9 copy.50
  (71 shorter events, 8.0 us)
Async XLA Ops:
  6.5 192.6 %copy-start = (bf16[128,2048]{1,0:T(8,128)(2,1)S(1)}, bf16[128,2048]{1,0:T(8,128)(2,1)}, u32[]{:S(2)}) copy-start(bf16[128,2048]{1,0:T(8,128)(2,1)} %param.18) | copy-start | bytes 1572868
  6.5 143.9 %all-gather.3.cloned.1.call-start = ((), (), s32[]{:S(2)}) async-start(), calls=%async_computation.4 | async-start | bytes 3194880 | tf_op jit(solution)/shard_map/all_gather | solution.py:31
  10.6 296.7 %all-gather.5.cloned.1.call-start = ((), (), s32[]{:S(2)}) async-start(), calls=%async_computation.5 | async-start | bytes 9052160 | tf_op jit(solution)/shard_map/all_gather | solution.py:17
  166.4 2.9 copy-start.1
  172.2 3.0 copy-start.1
  178.1 3.0 copy-start.1
  183.9 2.9 copy-start.1
  189.7 2.9 copy-start.1
  195.5 2.9 copy-start.1
  199.1 28.3 %copy-start.2 = (f32[2048]{0:T(1024)S(1)}, f32[2048]{0:T(1024)}, u32[]{:S(2)}) copy-start(f32[2048]{0:T(1024)} %param.20) | copy-start | bytes 24580
  200.4 25.8 %all-to-all-start = ((bf16[8,24,2048]{2,1,0:T(8,128)(2,1)}), bf16[8,24,2048]{2,1,0:T(8,128)(2,1)S(1)}, u32[]{:S(2)}, u32[]{:S(2)}) async-start(bf16[8,24,2048]{2,1,0:T(8,128)(2,1)} %bitcast.15), calls=%async_computation | async-start | bytes 1572864 | tf_op jit(solution)/shard_map/all_to_all | solution.py:42
Sparse Core Ops, SparseCore 0:
  10.7 139.7 all-gather.2
  153.4 153.7 all-gather.4
where the time goes:
time: 364 us; the launch traced here: 363 us
  waiting for transfers between devices  213 us (59%)
  blocking collectives  55.5 us (15%)
  matrix products  39.9 us (11%)
  local copies, waits for them, and re-layouts  19.8 us (5%)
  starting transfers between devices  13.7 us (4%)
  between operations  13.6 us (4%)
  other arithmetic  7.9 us (2%)
    all_gather x1, waiting for transfers between devices, in_one_piece(): lax.all_gather(both, axis, axis=dim, tiled=True)  136 us
    all_gather x1, waiting for transfers between devices, turned_gather(): lax.all_gather(both, axis, axis=0, tiled=True)  64.2 us
    all_to_all x2, blocking collectives, copy_for_each(): lax.all_to_all(jnp.broadcast_to(array[None], (peers, *array.shape)), axis...  31.1 us
    all_to_all x1, blocking collectives, summed_on_arrival(): lax.all_to_all(parts, axis, split_axis=0, concat_axis=0, tiled=True)  24.5 us
    dot_general x6, matrix products, absorb(): jnp.einsum('qgrk,kgd->qgrd', weight.astype(jnp.bfloat16), value_block, pr...  17 us
    dot_general x6, matrix products, absorb(): jnp.einsum('qgrd,kgd->qgrk', query_groups, key_block, preferred_element_t...  13.7 us
    all_to_all x1, starting transfers between devices, summed_on_arrival(): lax.all_to_all(parts, axis, split_axis=0, concat_axis=0, tiled=True)  13.7 us
    all_to_all x1, waiting for transfers between devices, summed_on_arrival(): lax.all_to_all(parts, axis, split_axis=0, concat_axis=0, tiled=True)  12.2 us
  transfers between devices with their start and end apart: 3, of which 3 were waited for; matrix products, arithmetic and copies ran while one was open for 15% of the time, Pallas kernels for 0%

commit v1 on v0

v1 whole, which is shorter than its diff:
```python
import functools
import jax
import jax.numpy as jnp
from jax import lax
from jax.sharding import PartitionSpec as P
from jax.experimental import pallas as pl
from jax.experimental.pallas import tpu as pltpu

GRID_W = 64
MESH = pl.DeviceIdType.MESH
epsilon = 1e-06
rope_base = 10000.0
Z, Y, X = 16, 4, 4
bf16, f32 = jnp.bfloat16, jnp.float32


def rotate_pairs(entries, places):
    half = entries.shape[-1] // 2
    frequency = rope_base ** (-jnp.arange(half, dtype=f32) / half)
    angle = places.astype(f32)[:, None, None] * frequency[None, None, :]
    cosine = jnp.cos(angle)
    sine = jnp.sin(angle)
    first = entries[..., :half]
    second = entries[..., half:]
    return jnp.concatenate(
        [first * cosine - second * sine, first * sine + second * cosine], axis=-1
    )


def grid_rotate(entries, grid_rows, grid_cols):
    half = entries.shape[-1] // 2
    return jnp.concatenate(
        [
            rotate_pairs(entries[..., :half], grid_rows),
            rotate_pairs(entries[..., half:], grid_cols),
        ],
        axis=-1,
    )


def head_norm(entries, gains):
    factor = lax.rsqrt(jnp.mean(entries * entries, axis=-1, keepdims=True) + epsilon)
    return entries * factor * gains[None]


def nt(a, b):
    return lax.dot_general(a, b, (((1,), (1,)), ((), ())), preferred_element_type=f32)


class Sems:
    def __init__(self):
        self.n = 0

    def __call__(self, count=1):
        at = self.n
        self.n += count
        return at


def plan():
    new = Sems()
    names = {}
    for name, count in (
        ("kvR", 8), ("kvL", 7), ("wR", 8), ("wL", 7), ("wD", 16), ("wy", 2), ("q", 3),
        ("res", 3), ("owx", 3), ("owd", 4), ("comb", 3), ("att", 32),
        ("ra1", 3), ("rb1", 3), ("ra2", 3), ("rb2", 3), ("outx", 3), ("outd", 4),
    ):
        names[name] = (new(count), new(count))
    names["local"] = (new(2), 0)
    return names, new.n


SEMS, NSEMS = plan()


def kernel(
    q_ref, kv_ref, wp_ref, ow_ref, res_ref, ng_ref, out_ref,
    kvb, qb, wb, owb, resb, oacc, macc, cs, cr, ao, att, mid, nrm, hid, part,
    rsa, rsb, a2, b2, rsa2, rsb2, sems,
):
    T = q_ref.shape[0]
    H = T // 2
    HH = H // 2
    D = out_ref.shape[1]
    DX = D // X
    K = kv_ref.shape[1]
    R = wp_ref.shape[2]
    sp = lax.axis_index("sp")
    tp = lax.axis_index("tp")
    z, y, x, c = sp // Y, sp % Y, tp // 2, tp % 2
    o = 1 - c

    def dev(z_, y_, x_, c_):
        return (z_ * Y + y_, x_ * 2 + c_)

    def ss(name, i=0):
        return sems.at[SEMS[name][0] + i]

    def rs(name, i=0):
        return sems.at[SEMS[name][1] + i]

    def remote(src, dst, name, i, to):
        return pltpu.make_async_remote_copy(
            src_ref=src, dst_ref=dst, send_sem=ss(name, i), recv_sem=rs(name, i),
            device_id=to, device_id_type=MESH,
        )

    def got(dst, name, i=0):
        pltpu.make_async_copy(dst, dst, rs(name, i)).wait()

    sent = []

    def go(copy):
        copy.start()
        sent.append(copy)

    barrier = pltpu.get_barrier_semaphore()
    me32 = y * 8 + tp

    def greet(k, _):
        other = lax.rem(me32 + k, 32)
        pl.semaphore_signal(
            barrier, inc=1, device_id=(z * Y + other // 8, other % 8), device_id_type=MESH
        )
        return 0

    lax.fori_loop(1, 32, greet, 0)
    zr, zl = lax.rem(z + 1, Z), lax.rem(z + Z - 1, Z)
    for zz in (zr, zl):
        pl.semaphore_signal(barrier, inc=1, device_id=dev(zz, y, x, c), device_id_type=MESH)
    pl.semaphore_wait(barrier, 33)

    def slot(k):
        return lax.rem(z + k + Z, Z)

    def kv_send(s):
        srcR = kv_ref if s == 0 else kvb.at[slot(-s)]
        go(remote(srcR, kvb.at[slot(-s)], "kvR", s, dev(zr, y, x, c)))
        if s < 7:
            srcL = kv_ref if s == 0 else kvb.at[slot(s)]
            go(remote(srcL, kvb.at[slot(s)], "kvL", s, dev(zl, y, x, c)))

    kv_send(0)
    for k in (1, 2, 3):
        yk = lax.rem(y + k, Y)
        go(remote(q_ref, qb.at[y], "q", k - 1, dev(z, yk, x, c)))
    wrow = pl.ds(pl.multiple_of((z * Y + y) * R, R), R)
    yc = y // 2
    for j in (0, 1):
        to = 2 * c + j
        own = jnp.logical_and(to == y, c == yc)
        src, dst = wp_ref.at[j], wb.at[:, wrow, :]
        far = pltpu.make_async_remote_copy(
            src_ref=src, dst_ref=dst, send_sem=ss("wy", j),
            recv_sem=sems.at[SEMS["wy"][1] + y % 2],
            device_id=dev(z, to, x, yc), device_id_type=MESH,
        )

        @pl.when(jnp.logical_not(own))
        def _():
            far.start()

        @pl.when(own)
        def _():
            pltpu.make_async_copy(src, dst, sems.at[SEMS["wy"][1] + y % 2]).start()

    owrow = pl.ds(pl.multiple_of(tp * 2 * 64, 128), 128)
    for k in (1, 2, 3):
        xk = lax.rem(x + k, X)
        go(remote(ow_ref, owb.at[owrow, :], "owx", k - 1, dev(z, y, xk, c)))
    go(remote(ow_ref, owb.at[owrow, :], "owd", 3, dev(z, y, x, o)))
    own_ow = pltpu.make_async_copy(ow_ref, owb.at[owrow, :], ss("local", 0))
    own_ow.start()
    half = pl.ds(pl.multiple_of(c * H, 32), H)
    own_rows = pl.ds(pl.multiple_of(y * H, 32), H)
    for k in (1, 2, 3):
        yk = lax.rem(y + k, Y)
        go(remote(res_ref.at[half, :], resb.at[own_rows, :], "res", k - 1, dev(z, yk, x, c)))
    own_res = pltpu.make_async_copy(res_ref.at[half, :], resb.at[own_rows, :], ss("local", 1))
    own_res.start()

    def wrows(k, core):
        return wb.at[:, pl.ds(pl.multiple_of((slot(k) * Y + 2 * core) * R, 2 * R), 2 * R), :]

    def w_ring(s):
        if s == 0:
            for i in (0, 1):
                yi = 2 * c + i
                row = pl.ds(pl.multiple_of((z * Y + yi) * R, R), R)
                pltpu.make_async_copy(
                    wb.at[:, row, :], wb.at[:, row, :], sems.at[SEMS["wy"][1] + i]
                ).wait()
        else:
            got(wrows(-s, c), "wR", s - 1)
            if s < 8:
                got(wrows(s, c), "wL", s - 1)
        if s < 8:
            go(remote(wrows(-s, c), wrows(-s, c), "wR", s, dev(zr, y, x, c)))
        if s < 7:
            go(remote(wrows(s, c), wrows(s, c), "wL", s, dev(zl, y, x, c)))
        go(remote(wrows(-s, c), wrows(-s, c), "wD", s, dev(z, y, x, o)))
        if 0 < s < 8:
            go(remote(wrows(s, c), wrows(s, c), "wD", 8 + s, dev(z, y, x, o)))

    def lanes(shape):
        return lax.broadcasted_iota(jnp.int32, shape, 1)

    def attend(blocks, first):
        k0, k1, v0, v1 = [], [], [], []
        for block in blocks:
            kv = block[...].astype(f32)
            turned = pltpu.roll(kv, K // 2, 1)
            low = lanes(kv.shape) < K // 2
            k0.append(jnp.where(low, kv, 0.0).astype(bf16))
            k1.append(jnp.where(low, 0.0, turned).astype(bf16))
            v0.append(jnp.where(low, turned, 1.0).astype(bf16))
            v1.append(jnp.where(low, 1.0, kv).astype(bf16))
        cat = lambda parts: parts[0] if len(parts) == 1 else jnp.concatenate(parts, axis=0)
        keys, vals = (cat(k0), cat(k1)), (cat(v0), cat(v1))

        def rows(j, _):
            q = qb[j]
            for h in (0, 1):
                score = nt(q, keys[h])
                top = jnp.max(score, axis=1, keepdims=True)
                if not first:
                    old = macc[h, j]
                    top = jnp.maximum(old, top)
                    weight = jnp.exp(score - top[:, :1])
                    total = jnp.dot(weight.astype(bf16), vals[h], preferred_element_type=f32)
                    oacc[h, j] = oacc[h, j] * jnp.exp(old - top) + total
                    macc[h, j] = top
                else:
                    weight = jnp.exp(score - top)
                    oacc[h, j] = jnp.dot(
                        weight.astype(bf16), vals[h], preferred_element_type=f32
                    )
                    macc[h, j] = jnp.broadcast_to(top, (T, K))
            return 0

        lax.fori_loop(0, Y, rows, 0)

    qb[y] = q_ref[...]
    for k in (1, 2, 3):
        got(qb.at[lax.rem(y + Y - k, Y)], "q", k - 1)
    w_ring(0)
    attend([kv_ref], True)
    wnext = 1
    for s in range(1, 9):
        got(kvb.at[slot(-s)], "kvR", s - 1)
        if s < 8:
            got(kvb.at[slot(s)], "kvL", s - 1)
            kv_send(s)
        attend([kvb.at[slot(-s)]] + ([kvb.at[slot(s)]] if s < 8 else []), False)
        if s in (2, 3, 4, 5, 6, 7):
            w_ring(wnext)
            wnext += 1

    low = lanes((T, K)) < K // 2
    even = (lanes((T, K)) // (K // 4)) % 2 == 0
    for j in range(Y):
        o0, o1 = oacc[0, j], oacc[1, j]
        total = jnp.where(low, pltpu.roll(o0, K // 2, 1), pltpu.roll(o1, K // 2, 1))
        level = jnp.where(low, macc[0, j], macc[1, j]) + jnp.log(total)
        high = level.astype(bf16)
        rest = (level - high.astype(f32)).astype(bf16)
        cs[j, 0] = (jnp.where(low, o0, o1) / total).astype(bf16)
        cs[j, 1] = jnp.where(even, high.astype(f32), rest.astype(f32)).astype(bf16)
    for k in (1, 2, 3):
        yk = lax.rem(y + k, Y)
        go(remote(cs.at[yk], cr.at[k - 1], "comb", k - 1, dev(z, yk, x, c)))
    w_ring(wnext)
    wnext += 1
    for k in (1, 2, 3):
        got(cr.at[k - 1], "comb", k - 1)

    def level_of(packed):
        wide = packed.astype(f32)
        return wide + jnp.where(
            even, pltpu.roll(wide, K - K // 4, 1), pltpu.roll(wide, K // 4, 1)
        )

    own = cs.at[y]
    outs = [own[0].astype(f32)] + [cr[k, 0].astype(f32) for k in range(3)]
    levels = [level_of(own[1])] + [level_of(cr[k, 1]) for k in range(3)]
    top = functools.reduce(jnp.maximum, levels)
    shares = [jnp.exp(v - top) for v in levels]
    total = sum(shares[1:], shares[0])
    summed = sum((a * b for a, b in zip(outs[1:], shares[1:])), outs[0] * shares[0])
    ao[...] = (summed / total).astype(bf16)

    my_cols = pl.ds(pl.multiple_of(tp * K, K), K)

    def att_copy(k):
        other = lax.rem(me32 + k, 32)
        oc = other % 2
        return remote(
            ao.at[pl.ds(pl.multiple_of(oc * H, 32), H), :], att.at[own_rows, my_cols],
            "att", k, (z * Y + other // 8, other % 8),
        )

    def att_send(k, _):
        att_copy(k).start()
        return 0

    lax.fori_loop(1, 32, att_send, 0)
    att[own_rows, my_cols] = ao[half, :]
    while wnext <= 8:
        w_ring(wnext)
        wnext += 1

    own_ow.wait()
    own_res.wait()
    for k in (1, 2, 3):
        xk = lax.rem(x + X - k, X)
        row = pl.ds(pl.multiple_of((xk * 2 + c) * 128, 128), 128)
        got(owb.at[row, :], "owx", k - 1)
        go(remote(owb.at[row, :], owb.at[row, :], "owd", k - 1, dev(z, y, x, o)))
    for k in (1, 2, 3):
        xk = lax.rem(x + X - k, X)
        got(owb.at[pl.ds(pl.multiple_of((xk * 2 + o) * 128, 128), 128), :], "owd", k - 1)
        yk = lax.rem(y + Y - k, Y)
        got(resb.at[pl.ds(pl.multiple_of(yk * H, 32), H), :], "res", k - 1)
    got(owb.at[pl.ds(pl.multiple_of((x * 2 + o) * 128, 128), 128), :], "owd", 3)

    def att_wait(k, _):
        other = lax.rem(me32 + 32 - k, 32)
        got(
            att.at[
                pl.ds(pl.multiple_of((other // 8) * H, 32), H),
                pl.ds(pl.multiple_of((other % 8) * K, K), K),
            ],
            "att", k,
        )
        return 0

    lax.fori_loop(1, 32, att_wait, 0)

    NB = 512

    def mid_cols(n, square):
        cols = pl.ds(pl.multiple_of(n * NB, NB), NB)
        branch = jnp.dot(att[...], owb[:, cols], preferred_element_type=f32)
        rounded = (resb[:, cols].astype(f32) + branch).astype(bf16)
        mid[:, cols] = rounded
        wide = rounded.astype(f32)
        wide = wide * wide
        return square + sum(wide[:, i * 128 : (i + 1) * 128] for i in range(NB // 128))

    square = lax.fori_loop(0, D // NB, mid_cols, jnp.zeros((Y * H, 128), f32))
    factor = lax.rsqrt(jnp.sum(square, axis=1, keepdims=True) * (1.0 / D) + epsilon)

    def norm_cols(n, _):
        cols = pl.ds(pl.multiple_of(n * NB, NB), NB)
        nrm[:, cols] = (mid[:, cols].astype(f32) * factor * ng_ref[:, cols]).astype(bf16)
        return 0

    lax.fori_loop(0, D // NB, norm_cols, 0)

    for s in range(9):
        got(wrows(-s, o), "wD", s)
        if 0 < s < 8:
            got(wrows(s, o), "wD", 8 + s)
    gate = jnp.dot(nrm[...], wb[0], preferred_element_type=f32)
    up = jnp.dot(nrm[...], wb[1], preferred_element_type=f32)
    hid[...] = (gate / (1.0 + jnp.exp(-gate)) * up).astype(bf16)

    def down_cols(n, _):
        cols = pl.ds(pl.multiple_of(n * NB, NB), NB)
        value = nt(hid[...], wb[2, cols, :]).astype(bf16)
        for j in range(Y):
            part[j, :, cols] = value[j * H : (j + 1) * H]
        return 0

    lax.fori_loop(0, D // NB, down_cols, 0)

    xcols = pl.ds(pl.multiple_of(x * DX, DX), DX)

    def cols_of(xk):
        return pl.ds(pl.multiple_of(xk * DX, DX), DX)

    for k in (1, 2, 3):
        yk = lax.rem(y + k, Y)
        xk = lax.rem(x + k, X)
        go(remote(part.at[yk, pl.ds(0, HH), :], rsa.at[k - 1], "ra1", k - 1, dev(z, yk, x, c)))
        go(
            remote(
                part.at[:, pl.ds(HH, HH), cols_of(xk)], rsb.at[k - 1], "rb1", k - 1,
                dev(z, y, xk, c),
            )
        )
    for k in (1, 2, 3):
        got(rsa.at[k - 1], "ra1", k - 1)
    a2[...] = (
        part[y, :HH, :].astype(f32)
        + rsa[0].astype(f32) + rsa[1].astype(f32) + rsa[2].astype(f32)
    ).astype(bf16)
    for k in (1, 2, 3):
        xk = lax.rem(x + k, X)
        go(remote(a2.at[:, cols_of(xk)], rsa2.at[k - 1], "ra2", k - 1, dev(z, y, xk, c)))
    for k in (1, 2, 3):
        got(rsb.at[k - 1], "rb1", k - 1)
    b2[...] = (
        part[:, HH:, xcols].astype(f32)
        + rsb[0].astype(f32) + rsb[1].astype(f32) + rsb[2].astype(f32)
    ).astype(bf16)
    for k in (1, 2, 3):
        yk = lax.rem(y + k, Y)
        go(remote(b2.at[yk], rsb2.at[k - 1], "rb2", k - 1, dev(z, yk, x, c)))
    for k in (1, 2, 3):
        got(rsa2.at[k - 1], "ra2", k - 1)
    top_rows = pl.ds(pl.multiple_of(c * H, 16), HH)
    low_rows = pl.ds(pl.multiple_of(c * H + HH, 16), HH)
    ffn = (
        a2[:, xcols].astype(f32)
        + rsa2[0].astype(f32) + rsa2[1].astype(f32) + rsa2[2].astype(f32)
    )
    mid_top = mid[pl.ds(pl.multiple_of(y * H, 16), HH), xcols]
    out_ref[top_rows, xcols] = (mid_top.astype(f32) + ffn).astype(bf16)
    for k in (1, 2, 3):
        got(rsb2.at[k - 1], "rb2", k - 1)
    ffn = b2[y].astype(f32) + rsb2[0].astype(f32) + rsb2[1].astype(f32) + rsb2[2].astype(f32)
    mid_low = mid[pl.ds(pl.multiple_of(y * H + HH, 16), HH), xcols]
    out_ref[low_rows, xcols] = (mid_low.astype(f32) + ffn).astype(bf16)

    mine = out_ref.at[half, xcols]
    for k in (1, 2, 3):
        xk = lax.rem(x + k, X)
        go(remote(mine, mine, "outx", k - 1, dev(z, y, xk, c)))
    go(remote(mine, mine, "outd", 3, dev(z, y, x, o)))
    for k in (1, 2, 3):
        piece = out_ref.at[half, cols_of(lax.rem(x + X - k, X))]
        got(piece, "outx", k - 1)
        go(remote(piece, piece, "outd", k - 1, dev(z, y, x, o)))
    other_half = pl.ds(pl.multiple_of(o * H, 32), H)
    for k in (1, 2, 3):
        got(out_ref.at[other_half, cols_of(lax.rem(x + X - k, X))], "outd", k - 1)
    got(out_ref.at[other_half, xcols], "outd", 3)

    for copy in sent:
        copy.wait_send()
    for j in (0, 1):
        to = 2 * c + j

        @pl.when(jnp.logical_not(jnp.logical_and(to == y, c == yc)))
        def _():
            pltpu.make_async_copy(wp_ref.at[j], wp_ref.at[j], ss("wy", j)).wait()

    def att_left(k, _):
        att_copy(k).wait_send()
        return 0

    lax.fori_loop(1, 32, att_left, 0)


def body(
    queries, keys, values, query_gain, key_gain, out_weight, residual, norm_gain,
    gate_weight, up_weight, down_weight,
):
    own = queries.shape[0]
    heads, head_size = query_gain.shape
    key_heads = key_gain.shape[0]
    places = lax.axis_index("sp") * own + jnp.arange(own, dtype=jnp.int32)
    grid_rows = places // GRID_W
    grid_cols = places % GRID_W
    scale = head_size ** (-0.5)
    q = grid_rotate(
        head_norm(queries.astype(f32).reshape(own, heads, head_size), query_gain),
        grid_rows, grid_cols,
    )
    q = (q.astype(bf16) * scale).astype(bf16).reshape(own, heads * head_size)
    k = (
        grid_rotate(
            head_norm(keys.astype(f32).reshape(own, key_heads, head_size), key_gain),
            grid_rows, grid_cols,
        )
        .astype(bf16)
        .reshape(own, key_heads * head_size)
    )
    kv = jnp.concatenate([k, values], axis=1)
    units = gate_weight.shape[1] // 2
    rows = gate_weight.shape[0]
    both = jnp.stack([gate_weight, up_weight, down_weight.T])
    both = both.reshape(3, rows, 2, units)
    padded = -(-units // 128) * 128
    both = jnp.pad(both, ((0, 0), (0, 0), (0, 0), (0, padded - units)))
    pieces = jnp.moveaxis(both, 2, 0)
    D = residual.shape[1]
    T, H, K = own, own // 2, kv.shape[1]
    HH, DX = H // 2, D // X
    vmem = pl.BlockSpec(memory_space=pltpu.VMEM)
    hbm = pl.BlockSpec(memory_space=pl.ANY)
    return pl.pallas_call(
        kernel,
        out_shape=jax.ShapeDtypeStruct((own, D), bf16),
        in_specs=[vmem, vmem, vmem, hbm, hbm, vmem],
        out_specs=vmem,
        scratch_shapes=[
            pltpu.VMEM((Z, T, K), bf16),
            pltpu.VMEM((Y, T, K), bf16),
            pltpu.VMEM((3, D, padded), bf16),
            pltpu.VMEM((8 * K, D), bf16),
            pltpu.VMEM((Y * H, D), bf16),
            pltpu.VMEM((2, Y, T, K), f32),
            pltpu.VMEM((2, Y, T, K), f32),
            pltpu.VMEM((Y, 2, T, K), bf16),
            pltpu.VMEM((3, 2, T, K), bf16),
            pltpu.VMEM((T, K), bf16),
            pltpu.VMEM((Y * H, 8 * K), bf16),
            pltpu.VMEM((Y * H, D), bf16),
            pltpu.VMEM((Y * H, D), bf16),
            pltpu.VMEM((Y * H, padded), bf16),
            pltpu.VMEM((Y, H, D), bf16),
            pltpu.VMEM((3, HH, D), bf16),
            pltpu.VMEM((3, Y, HH, DX), bf16),
            pltpu.VMEM((HH, D), bf16),
            pltpu.VMEM((Y, HH, DX), bf16),
            pltpu.VMEM((3, HH, DX), bf16),
            pltpu.VMEM((3, HH, DX), bf16),
            pltpu.SemaphoreType.DMA((NSEMS,)),
        ],
        compiler_params=pltpu.CompilerParams(
            collective_id=0, has_side_effects=True, vmem_limit_bytes=60 * 1024 * 1024
        ),
    )(q, kv, pieces, out_weight, residual, norm_gain.reshape(1, D))


def solution(mesh):
    in_specs = (
        P("sp", "tp"), P("sp", "tp"), P("sp", "tp"), P("tp", None), P("tp", None),
        P("tp", None), P("sp", None), P(), P("sp", "tp"), P("sp", "tp"), P("tp", "sp"),
    )
    return jax.shard_map(
        body, mesh=mesh, in_specs=in_specs, out_specs=P("sp", None), check_vma=False
    )
```

time: 364 us -> 135 us (0.37)
  waiting for transfers between devices: 213 us -> 0 us
  Pallas kernels: 0 us -> 123 us
  blocking collectives: 55.5 us -> 0 us
  matrix products: 39.9 us -> 0 us
  starting transfers between devices: 13.7 us -> 0 us
  between operations: 13.6 us -> 0.15 us
  local copies, waits for them, and re-layouts: 19.8 us -> 9.34 us
  other arithmetic: 7.9 us -> 2.12 us
    all_gather x2 -> x0, waiting for transfers between devices: 200 us -> none  [the longest x1 136 us: in_one_piece(): lax.all_gather(both, axis, axis=dim, tiled=True)]
    pallas_call x0 -> x1, Pallas kernels: none -> 123 us  [body(): pl.pallas_call(kernel, out_shape=jax.ShapeDtypeStruct((own, D), bf16), in...]
    all_to_all x3 -> x0, blocking collectives: 55.5 us -> none  [the longest x2 31.1 us: copy_for_each(): lax.all_to_all(jnp.broadcast_to(array[None], (peers, *array.shape)), axis...]
    dot_general x15 -> x0, matrix products: 39.9 us -> none  [the longest x6 17 us: absorb(): jnp.einsum('qgrk,kgd->qgrd', weight.astype(jnp.bfloat16), value_block, pr...]
    all_to_all x1 -> x0, starting transfers between devices: 13.7 us -> none  [summed_on_arrival(): lax.all_to_all(parts, axis, split_axis=0, concat_axis=0, tiled=True)]
    all_to_all x1 -> x0, waiting for transfers between devices: 12.2 us -> none  [summed_on_arrival(): lax.all_to_all(parts, axis, split_axis=0, concat_axis=0, tiled=True)]
    split x1 -> x0, local copies, waits for them, and re-layouts: 6.21 us -> none  [in_one_piece(): jnp.split(lax.all_gather(both, axis, axis=dim, tiled=True), ends, axis=al...]
    reduce_sum x9 -> x0, other arithmetic: 4.65 us -> none  [the longest x6 3.4 us: absorb(): total = total * shrink + jnp.sum(weight, axis=-1)]
  transfers between devices with their start and end apart: 3 -> 0, of which waited for: 3 -> 0; matrix products, arithmetic and copies ran while one was open for 15% -> 0% of each run, Pallas kernels for 0% -> 0%
where the time goes in v1:
time: 135 us; the launch traced here: 134 us
  Pallas kernels  123 us (91%)
  local copies, waits for them, and re-layouts  9.34 us (7%)
  other arithmetic  2.12 us (2%)
    pallas_call x1, Pallas kernels, body(): pl.pallas_call(kernel, out_shape=jax.ShapeDtypeStruct((own, D), bf16), in...  123 us
    unnamed x18, local copies, waits for them, and re-layouts  7.47 us

profile of v1, /device:TPU:1, one launch (start us, length us, event | category | flops | bytes accessed | tf_op | source)
XLA Modules:
  0.0 134.3 jit_solution(7278434953658357016)
XLA Ops:
  0.0 0.9 copy.22
  0.9 0.1 fusion.16
  1.0 0.0 copy-start.6
  1.0 0.6 copy-done.6
  1.7 0.0 copy-start.4
  1.7 0.1 fusion.18
  1.8 0.7 copy-done.4
  2.4 0.0 copy-start.1
  2.4 0.1 copy.25
  2.6 0.7 copy-done.1
  3.2 0.1 stack.12
  3.4 0.0 copy-start.2
  3.4 0.8 copy-done.2
  4.2 0.1 stack.13
  4.3 0.0 copy-start.3
  4.3 0.8 copy-done.3
  5.1 0.1 stack.14
  5.2 0.0 copy-start
  5.2 0.7 fusion.5.wp_ref
  5.9 0.1 copy-done
  6.0 0.1 copy.21
  6.2 0.0 copy-start.5
  6.2 0.7 copy-done.5
  6.9 0.1 fusion.15
  6.9 0.2 multiply_cosine_fusion.3
  7.2 0.7 copy.29.q_ref
  7.9 0.8 fusion.29
  8.8 0.8 concatenate.27.kv_ref
  9.5 122.7 %shard_map.109 = bf16[192,2048]{1,0:T(8,128)(2,1)} custom-call(bf16[192,128]{1,0:T(8,128)(2,1)} %copy.29.q_ref, bf16[192,128]{1,0:T(8,128)(2,1)} %concatenate.27.kv_ref, bf16[2,3,32,384]{3,2,1,0:T(8,128)(2,1)} %fusion.5.wp_ref, bf16[128,2048]{1,0:T(8,128)(2,1)} %ow_ref.1, bf16[192,2048]{1,0:T(8,128)(2,1)} %res_ref.1, f32[1,2048]{1,0:T(1,128)} %bitcast.22), custom_call_target="tpu_custom_call" | custom-call | tf_op jit(solution)/shard_map/pallas_call | solution.py:493
  132.2 2.1 %copy.31 = bf16[192,2048]{1,0:T(8,128)(2,1)} copy(bf16[192,2048]{1,0:T(8,128)(2,1)} %shard_map.109) | data formatting | bytes 1572864
  (10 shorter events, 0.1 us)
Async XLA Ops:
  1.0 0.7 copy-start.6
  1.7 0.8 copy-start.4
  2.4 0.8 copy-start.1
  3.4 0.8 copy-start.2
  4.3 0.8 copy-start.3
  5.2 0.8 copy-start
  6.2 0.7 copy-start.5

commit v2 on v1

--- a/solution.py
+++ b/solution.py
@@ -1,6 +1,7 @@
 import functools
 import jax
 import jax.numpy as jnp
+import numpy as np
 from jax import lax
 from jax.sharding import PartitionSpec as P
 from jax.experimental import pallas as pl
@@ -14,33 +15,13 @@
 bf16, f32 = jnp.bfloat16, jnp.float32
 
 
-def rotate_pairs(entries, places):
-    half = entries.shape[-1] // 2
-    frequency = rope_base ** (-jnp.arange(half, dtype=f32) / half)
-    angle = places.astype(f32)[:, None, None] * frequency[None, None, :]
-    cosine = jnp.cos(angle)
-    sine = jnp.sin(angle)
-    first = entries[..., :half]
-    second = entries[..., half:]
-    return jnp.concatenate(
-        [first * cosine - second * sine, first * sine + second * cosine], axis=-1
-    )
-
-
-def grid_rotate(entries, grid_rows, grid_cols):
-    half = entries.shape[-1] // 2
-    return jnp.concatenate(
-        [
-            rotate_pairs(entries[..., :half], grid_rows),
-            rotate_pairs(entries[..., half:], grid_cols),
-        ],
-        axis=-1,
-    )
-
-
-def head_norm(entries, gains):
-    factor = lax.rsqrt(jnp.mean(entries * entries, axis=-1, keepdims=True) + epsilon)
-    return entries * factor * gains[None]
+def rope_tables(count, head_size, width):
+    half = head_size // 2
+    pairs = half // 2
+    lane = np.arange(width) % half
+    angle = np.arange(count)[:, None] * rope_base ** (-(lane % pairs) / pairs)[None, :]
+    sine = np.where(lane[None, :] < pairs, -np.sin(angle), np.sin(angle))
+    return np.stack([np.cos(angle), sine]).astype(np.float32)
 
 
 def nt(a, b):
@@ -61,20 +42,28 @@
     new = Sems()
     names = {}
     for name, count in (
-        ("kvR", 8), ("kvL", 7), ("wR", 8), ("wL", 7), ("wD", 16), ("wy", 2), ("q", 3),
+        ("kvR", 8), ("kvL", 7), ("wR", 24), ("wL", 21), ("wD", 16), ("wE", 16), ("wy", 2), ("q", 3),
         ("res", 3), ("owx", 3), ("owd", 4), ("comb", 3), ("att", 32),
-        ("ra1", 3), ("rb1", 3), ("ra2", 3), ("rb2", 3), ("outx", 3), ("outd", 4),
+        ("ra1", 12), ("rb1", 3), ("ra2", 3), ("rb2", 3), ("outx", 3), ("outd", 4),
     ):
         names[name] = (new(count), new(count))
     names["local"] = (new(2), 0)
+    names["in"] = (new(10), 0)
     return names, new.n
 
 
 SEMS, NSEMS = plan()
+W_AT = (2, 2, 1, 2)
+W_COMB = 3
+W_ATT = 9
+W_GATE = 0
 
 
 def kernel(
-    q_ref, kv_ref, wp_ref, ow_ref, res_ref, ng_ref, out_ref,
+    q_in, k_in, v_in, qg_in, kg_in, gate_in, up_in, down_in, tab_in,
+    ow_ref, res_ref, ng_in, out_ref,
+    q_raw, k_raw, v_raw, qg_raw, kg_raw, w_raw, tab, ng_ref,
+    q_ref, kv_ref, wp_ref,
     kvb, qb, wb, owb, resb, oacc, macc, cs, cr, ao, att, mid, nrm, hid, part,
     rsa, rsb, a2, b2, rsa2, rsb2, sems,
 ):
@@ -114,6 +103,20 @@
         copy.start()
         sent.append(copy)
 
+    ins = [
+        pltpu.make_async_copy(src, dst, ss("in", i))
+        for i, (src, dst) in enumerate(
+            (
+                (k_in, k_raw), (v_in, v_raw), (kg_in, kg_raw), (tab_in, tab),
+                (q_in, q_raw), (qg_in, qg_raw),
+                (gate_in, w_raw.at[0]), (up_in, w_raw.at[1]), (down_in, w_raw.at[2]),
+                (ng_in, ng_ref),
+            )
+        )
+    ]
+    for copy in ins:
+        copy.start()
+
     barrier = pltpu.get_barrier_semaphore()
     me32 = y * 8 + tp
 
@@ -126,24 +129,81 @@
 
     lax.fori_loop(1, 32, greet, 0)
     zr, zl = lax.rem(z + 1, Z), lax.rem(z + Z - 1, Z)
-    for zz in (zr, zl):
+    zr2, zl2 = lax.rem(z + 2, Z), lax.rem(z + Z - 2, Z)
+    for zz in (zr, zl, zr2, zl2):
         pl.semaphore_signal(barrier, inc=1, device_id=dev(zz, y, x, c), device_id_type=MESH)
-    pl.semaphore_wait(barrier, 33)
+
+    def lanes(shape):
+        return lax.broadcasted_iota(jnp.int32, shape, 1)
+
+    S = K // 2
+    lane = lanes((T, K))
+    rows_in = T // GRID_W
+
+    def table(i):
+        by_row = [
+            jnp.broadcast_to(tab[i, pl.ds(sp * rows_in + r, 1), :], (GRID_W, K))
+            for r in range(rows_in)
+        ]
+        by_col = jnp.concatenate([tab[i, :GRID_W, :]] * rows_in, axis=0)
+        return jnp.where(lane % S < S // 2, jnp.concatenate(by_row, axis=0), by_col)
+
+    def turn(wide, gain):
+        square = wide * wide
+        low_sum = jnp.sum(jnp.where(lane < S, square, 0.0), axis=1, keepdims=True)
+        high_sum = jnp.sum(jnp.where(lane < S, 0.0, square), axis=1, keepdims=True)
+        mean = jnp.where(lane < S, low_sum, high_sum) * (1.0 / S)
+        normed = wide * lax.rsqrt(mean + epsilon) * gain
+        pairs = S // 4
+        partner = jnp.where(
+            lane % (2 * pairs) < pairs,
+            pltpu.roll(normed, K - pairs, 1), pltpu.roll(normed, pairs, 1),
+        )
+        return (normed * cosine + partner * sine).astype(bf16)
+
+    for copy in ins[:4]:
+        copy.wait()
+    cosine, sine = table(0), table(1)
+    kv = jnp.concatenate([k_raw[...].astype(f32), v_raw[...].astype(f32)], axis=0).T
+    key_gain = jnp.concatenate([kg_raw[...], kg_raw[...]], axis=1)
+    key_turned = turn(kv, key_gain).astype(f32)
+    kv_ref[...] = jnp.where(lane < S, key_turned, kv).astype(bf16)
+    pl.semaphore_wait(barrier, 35)
 
     def slot(k):
         return lax.rem(z + k + Z, Z)
 
-    def kv_send(s):
-        srcR = kv_ref if s == 0 else kvb.at[slot(-s)]
-        go(remote(srcR, kvb.at[slot(-s)], "kvR", s, dev(zr, y, x, c)))
-        if s < 7:
-            srcL = kv_ref if s == 0 else kvb.at[slot(s)]
-            go(remote(srcL, kvb.at[slot(s)], "kvL", s, dev(zl, y, x, c)))
+    def kv_send(i):
+        left, right = kvb.at[slot(2 * i)], kvb.at[slot(-2 * i)]
+        srcL, srcR = (kv_ref, kv_ref) if i == 0 else (left, right)
+        go(remote(srcR, right, "kvR", 2 * i + 1, dev(zr2, y, x, c)))
+        if i < 3:
+            go(remote(srcL, left, "kvL", 2 * i + 1, dev(zl2, y, x, c)))
+        go(remote(srcR, right, "kvR", 2 * i, dev(zr, y, x, c)))
+        go(remote(srcL, left, "kvL", 2 * i, dev(zl, y, x, c)))
 
     kv_send(0)
+    for copy in ins[4:6]:
+        copy.wait()
+    query_gain = jnp.concatenate([qg_raw[0:1, :], qg_raw[1:2, :]], axis=1)
+    query = turn(q_raw[...].astype(f32), query_gain).astype(f32) * (S ** -0.5)
+    q_ref[...] = query.astype(bf16)
+    qb[y] = q_ref[...]
     for k in (1, 2, 3):
         yk = lax.rem(y + k, Y)
         go(remote(q_ref, qb.at[y], "q", k - 1, dev(z, yk, x, c)))
+    for copy in ins[6:]:
+        copy.wait()
+    units, padded = w_raw.shape[2] // 2, wp_ref.shape[3]
+    wide_lane = lanes((R, padded))
+    for m in range(3):
+        raw = w_raw[m].astype(f32)
+        low_part = jnp.where(wide_lane < units, raw[:, :padded], 0.0)
+        high_part = jnp.concatenate(
+            [raw[:, units:], jnp.zeros((R, padded - units), f32)], axis=1
+        )
+        wp_ref[0, m] = low_part.astype(bf16)
+        wp_ref[1, m] = high_part.astype(bf16)
     wrow = pl.ds(pl.multiple_of((z * Y + y) * R, R), R)
     yc = y // 2
     for j in (0, 1):
@@ -173,37 +233,62 @@
     own_ow.start()
     half = pl.ds(pl.multiple_of(c * H, 32), H)
     own_rows = pl.ds(pl.multiple_of(y * H, 32), H)
-    for k in (1, 2, 3):
-        yk = lax.rem(y + k, Y)
-        go(remote(res_ref.at[half, :], resb.at[own_rows, :], "res", k - 1, dev(z, yk, x, c)))
     own_res = pltpu.make_async_copy(res_ref.at[half, :], resb.at[own_rows, :], ss("local", 1))
     own_res.start()
 
-    def wrows(k, core):
-        return wb.at[:, pl.ds(pl.multiple_of((slot(k) * Y + 2 * core) * R, 2 * R), 2 * R), :]
-
-    def w_ring(s):
-        if s == 0:
+    def res_send():
+        for k in (1, 2, 3):
+            yk = lax.rem(y + k, Y)
+            go(remote(res_ref.at[half, :], resb.at[own_rows, :], "res", k - 1, dev(z, yk, x, c)))
+
+    res_send()
+
+    def wrows(k, core, m=None):
+        rows = pl.ds(pl.multiple_of((slot(k) * Y + 2 * core) * R, 2 * R), 2 * R)
+        return wb.at[:, rows, :] if m is None else wb.at[m, rows, :]
+
+    def w_shared(k, core, m):
+        rows = pl.ds(pl.multiple_of((slot(k) * Y + 2 * core) * R, 2 * R), 2 * R)
+        return wb.at[pl.ds(0, 2) if m == 1 else pl.ds(2, 1), rows, :]
+
+    def w_unit(s, m):
+        if s == 0 and m == 0:
             for i in (0, 1):
                 yi = 2 * c + i
                 row = pl.ds(pl.multiple_of((z * Y + yi) * R, R), R)
                 pltpu.make_async_copy(
                     wb.at[:, row, :], wb.at[:, row, :], sems.at[SEMS["wy"][1] + i]
                 ).wait()
-        else:
-            got(wrows(-s, c), "wR", s - 1)
-            if s < 8:
-                got(wrows(s, c), "wL", s - 1)
+        if s > 0:
+            got(wrows(-s, c, m), "wR", 3 * (s - 1) + m)
         if s < 8:
-            go(remote(wrows(-s, c), wrows(-s, c), "wR", s, dev(zr, y, x, c)))
+            block = wrows(-s, c, m)
+            go(remote(block, block, "wR", 3 * s + m, dev(zr, y, x, c)))
+        if 0 < s < 8:
+            got(wrows(s, c, m), "wL", 3 * (s - 1) + m)
         if s < 7:
-            go(remote(wrows(s, c), wrows(s, c), "wL", s, dev(zl, y, x, c)))
-        go(remote(wrows(-s, c), wrows(-s, c), "wD", s, dev(z, y, x, o)))
-        if 0 < s < 8:
-            go(remote(wrows(s, c), wrows(s, c), "wD", 8 + s, dev(z, y, x, o)))
-
-    def lanes(shape):
-        return lax.broadcasted_iota(jnp.int32, shape, 1)
+            block = wrows(s, c, m)
+            go(remote(block, block, "wL", 3 * s + m, dev(zl, y, x, c)))
+        if m > 0:
+            for i, k in ((s, -s), (8 + s, s)):
+                if i > 8 and not 0 < s < 8 or i == 8 and s == 0:
+                    continue
+                share = w_shared(k, c, m)
+                go(remote(share, share, "wD" if m == 1 else "wE", i, dev(z, y, x, o)))
+
+    order = [(s + 2 * (m == 2), m, s) for s in range(9) for m in range(3)]
+    todo_units = [(s, m) for _, m, s in sorted(order)]
+
+    def w_units(count):
+        for unit in todo_units[:count]:
+            w_unit(*unit)
+        del todo_units[:count]
+
+    def ow_pass(k):
+        xk = lax.rem(x + X - k, X)
+        row = pl.ds(pl.multiple_of((xk * 2 + c) * 128, 128), 128)
+        got(owb.at[row, :], "owx", k - 1)
+        go(remote(owb.at[row, :], owb.at[row, :], "owd", k - 1, dev(z, y, x, o)))
 
     def attend(blocks, first):
         k0, k1, v0, v1 = [], [], [], []
@@ -218,50 +303,56 @@
         cat = lambda parts: parts[0] if len(parts) == 1 else jnp.concatenate(parts, axis=0)
         keys, vals = (cat(k0), cat(k1)), (cat(v0), cat(v1))
 
-        def rows(j, _):
-            q = qb[j]
-            for h in (0, 1):
-                score = nt(q, keys[h])
-                top = jnp.max(score, axis=1, keepdims=True)
-                if not first:
-                    old = macc[h, j]
-                    top = jnp.maximum(old, top)
-                    weight = jnp.exp(score - top[:, :1])
-                    total = jnp.dot(weight.astype(bf16), vals[h], preferred_element_type=f32)
-                    oacc[h, j] = oacc[h, j] * jnp.exp(old - top) + total
-                    macc[h, j] = top
-                else:
-                    weight = jnp.exp(score - top)
-                    oacc[h, j] = jnp.dot(
-                        weight.astype(bf16), vals[h], preferred_element_type=f32
-                    )
-                    macc[h, j] = jnp.broadcast_to(top, (T, K))
-            return 0
-
-        lax.fori_loop(0, Y, rows, 0)
-
-    qb[y] = q_ref[...]
-    for k in (1, 2, 3):
-        got(qb.at[lax.rem(y + Y - k, Y)], "q", k - 1)
-    w_ring(0)
-    attend([kv_ref], True)
-    wnext = 1
-    for s in range(1, 9):
-        got(kvb.at[slot(-s)], "kvR", s - 1)
-        if s < 8:
-            got(kvb.at[slot(s)], "kvL", s - 1)
-            kv_send(s)
-        attend([kvb.at[slot(-s)]] + ([kvb.at[slot(s)]] if s < 8 else []), False)
-        if s in (2, 3, 4, 5, 6, 7):
-            w_ring(wnext)
-            wnext += 1
+        n = keys[0].shape[0]
+        todo = [(h, j) for j in range(Y * T // RB) for h in (0, 1)]
+
+        def scores(h, j):
+            q = qb[j * RB // T : (j + 1) * RB // T].reshape(RB, K)
+            return nt(q, keys[h])
+
+        ahead = scores(*todo[0])
+        for i, (h, j) in enumerate(todo):
+            score = ahead
+            if i + 1 < len(todo):
+                ahead = scores(*todo[i + 1])
+            rows = pl.ds(j * RB, RB)
+            top = jnp.broadcast_to(jnp.max(score, axis=1, keepdims=True), (RB, K))
+            if not first:
+                old = macc[h, rows]
+                top = jnp.maximum(old, top)
+            wide = [top] * (n // K) + ([top[:, : n % K]] if n % K else [])
+            weight = jnp.exp(score - jnp.concatenate(wide, axis=1))
+            total = jnp.dot(weight.astype(bf16), vals[h], preferred_element_type=f32)
+            if not first:
+                total = oacc[h, rows] * jnp.exp(old - top) + total
+            oacc[h, rows] = total
+            macc[h, rows] = top
+
+    RB = 2 * T
+    for i in range(4):
+        near, far = 2 * i + 1, 2 * i + 2
+        got(kvb.at[slot(-far)], "kvR", far - 1)
+        if i < 3:
+            got(kvb.at[slot(far)], "kvL", far - 1)
+            kv_send(i + 1)
+        got(kvb.at[slot(-near)], "kvR", near - 1)
+        got(kvb.at[slot(near)], "kvL", near - 1)
+        if i == 0:
+            for k in (1, 2, 3):
+                got(qb.at[lax.rem(y + Y - k, Y)], "q", k - 1)
+        blocks = [kvb.at[slot(k)] for k in ((-near, near, -far, far) if i < 3 else (-near, near, -far))]
+        if i == 0:
+            attend([kv_ref], True)
+        attend(blocks, False)
+        w_units(W_AT[i])
 
     low = lanes((T, K)) < K // 2
     even = (lanes((T, K)) // (K // 4)) % 2 == 0
     for j in range(Y):
-        o0, o1 = oacc[0, j], oacc[1, j]
+        rows = pl.ds(j * T, T)
+        o0, o1 = oacc[0, rows], oacc[1, rows]
         total = jnp.where(low, pltpu.roll(o0, K // 2, 1), pltpu.roll(o1, K // 2, 1))
-        level = jnp.where(low, macc[0, j], macc[1, j]) + jnp.log(total)
+        level = jnp.where(low, macc[0, rows], macc[1, rows]) + jnp.log(total)
         high = level.astype(bf16)
         rest = (level - high.astype(f32)).astype(bf16)
         cs[j, 0] = (jnp.where(low, o0, o1) / total).astype(bf16)
@@ -269,8 +360,7 @@
     for k in (1, 2, 3):
         yk = lax.rem(y + k, Y)
         go(remote(cs.at[yk], cr.at[k - 1], "comb", k - 1, dev(z, yk, x, c)))
-    w_ring(wnext)
-    wnext += 1
+    w_units(W_COMB)
     for k in (1, 2, 3):
         got(cr.at[k - 1], "comb", k - 1)
 
@@ -305,17 +395,12 @@
 
     lax.fori_loop(1, 32, att_send, 0)
     att[own_rows, my_cols] = ao[half, :]
-    while wnext <= 8:
-        w_ring(wnext)
-        wnext += 1
+    for k in (1, 2, 3):
+        ow_pass(k)
+    w_units(W_ATT)
 
     own_ow.wait()
     own_res.wait()
-    for k in (1, 2, 3):
-        xk = lax.rem(x + X - k, X)
-        row = pl.ds(pl.multiple_of((xk * 2 + c) * 128, 128), 128)
-        got(owb.at[row, :], "owx", k - 1)
-        go(remote(owb.at[row, :], owb.at[row, :], "owd", k - 1, dev(z, y, x, o)))
     for k in (1, 2, 3):
         xk = lax.rem(x + X - k, X)
         got(owb.at[pl.ds(pl.multiple_of((xk * 2 + o) * 128, 128), 128), :], "owd", k - 1)
@@ -339,7 +424,7 @@
     NB = 512
 
     def mid_cols(n, square):
-        cols = pl.ds(pl.multiple_of(n * NB, NB), NB)
+        cols = pl.ds(n * NB, NB)
         branch = jnp.dot(att[...], owb[:, cols], preferred_element_type=f32)
         rounded = (resb[:, cols].astype(f32) + branch).astype(bf16)
         mid[:, cols] = rounded
@@ -347,7 +432,10 @@
         wide = wide * wide
         return square + sum(wide[:, i * 128 : (i + 1) * 128] for i in range(NB // 128))
 
-    square = lax.fori_loop(0, D // NB, mid_cols, jnp.zeros((Y * H, 128), f32))
+    square = jnp.zeros((Y * H, 128), f32)
+    for n in range(D // NB):
+        square = mid_cols(n, square)
+        w_units(1)
     factor = lax.rsqrt(jnp.sum(square, axis=1, keepdims=True) * (1.0 / D) + epsilon)
 
     def norm_cols(n, _):
@@ -357,40 +445,53 @@
 
     lax.fori_loop(0, D // NB, norm_cols, 0)
 
-    for s in range(9):
-        got(wrows(-s, o), "wD", s)
-        if 0 < s < 8:
-            got(wrows(s, o), "wD", 8 + s)
+    w_units(W_GATE)
+
+    def shared_in(m, name):
+        for s in range(9):
+            got(w_shared(-s, o, m), name, s)
+            if 0 < s < 8:
+                got(w_shared(s, o, m), name, 8 + s)
+
+    while any(m < 2 for _, m in todo_units):
+        w_units(1)
+    shared_in(1, "wD")
     gate = jnp.dot(nrm[...], wb[0], preferred_element_type=f32)
     up = jnp.dot(nrm[...], wb[1], preferred_element_type=f32)
     hid[...] = (gate / (1.0 + jnp.exp(-gate)) * up).astype(bf16)
 
-    def down_cols(n, _):
-        cols = pl.ds(pl.multiple_of(n * NB, NB), NB)
+    w_units(len(todo_units))
+    shared_in(2, "wE")
+
+    xcols = pl.ds(pl.multiple_of(x * DX, DX), DX)
+
+    def cols_of(xk):
+        return pl.ds(pl.multiple_of(xk * DX, DX), DX)
+
+    for k in (1, 2, 3, 4):
+        xk = lax.rem(x + k, X)
+        cols = cols_of(xk)
         value = nt(hid[...], wb[2, cols, :]).astype(bf16)
         for j in range(Y):
             part[j, :, cols] = value[j * H : (j + 1) * H]
-        return 0
-
-    lax.fori_loop(0, D // NB, down_cols, 0)
-
-    xcols = pl.ds(pl.multiple_of(x * DX, DX), DX)
-
-    def cols_of(xk):
-        return pl.ds(pl.multiple_of(xk * DX, DX), DX)
-
-    for k in (1, 2, 3):
-        yk = lax.rem(y + k, Y)
-        xk = lax.rem(x + k, X)
-        go(remote(part.at[yk, pl.ds(0, HH), :], rsa.at[k - 1], "ra1", k - 1, dev(z, yk, x, c)))
-        go(
-            remote(
-                part.at[:, pl.ds(HH, HH), cols_of(xk)], rsb.at[k - 1], "rb1", k - 1,
-                dev(z, y, xk, c),
+        if k < 4:
+            go(
+                remote(
+                    part.at[:, pl.ds(HH, HH), cols], rsb.at[k - 1], "rb1", k - 1,
+                    dev(z, y, xk, c),
+                )
             )
-        )
-    for k in (1, 2, 3):
-        got(rsa.at[k - 1], "ra1", k - 1)
+        for i in (1, 2, 3):
+            yk = lax.rem(y + i, Y)
+            go(
+                remote(
+                    part.at[yk, pl.ds(0, HH), cols], rsa.at[i - 1, :, cols],
+                    "ra1", 4 * (i - 1) + k - 1, dev(z, yk, x, c),
+                )
+            )
+    for k in (1, 2, 3):
+        for i in range(4):
+            got(rsa.at[k - 1, :, cols_of(lax.rem(x + i + 1, X))], "ra1", 4 * (k - 1) + i)
     a2[...] = (
         part[y, :HH, :].astype(f32)
         + rsa[0].astype(f32) + rsa[1].astype(f32) + rsa[2].astype(f32)
@@ -458,51 +559,40 @@
     gate_weight, up_weight, down_weight,
 ):
     own = queries.shape[0]
-    heads, head_size = query_gain.shape
-    key_heads = key_gain.shape[0]
-    places = lax.axis_index("sp") * own + jnp.arange(own, dtype=jnp.int32)
-    grid_rows = places // GRID_W
-    grid_cols = places % GRID_W
-    scale = head_size ** (-0.5)
-    q = grid_rotate(
-        head_norm(queries.astype(f32).reshape(own, heads, head_size), query_gain),
-        grid_rows, grid_cols,
-    )
-    q = (q.astype(bf16) * scale).astype(bf16).reshape(own, heads * head_size)
-    k = (
-        grid_rotate(
-            head_norm(keys.astype(f32).reshape(own, key_heads, head_size), key_gain),
-            grid_rows, grid_cols,
-        )
-        .astype(bf16)
-        .reshape(own, key_heads * head_size)
-    )
-    kv = jnp.concatenate([k, values], axis=1)
-    units = gate_weight.shape[1] // 2
-    rows = gate_weight.shape[0]
-    both = jnp.stack([gate_weight, up_weight, down_weight.T])
-    both = both.reshape(3, rows, 2, units)
-    padded = -(-units // 128) * 128
-    both = jnp.pad(both, ((0, 0), (0, 0), (0, 0), (0, padded - units)))
-    pieces = jnp.moveaxis(both, 2, 0)
+    head_size = query_gain.shape[1]
+    K = queries.shape[1]
+    tables = jnp.asarray(rope_tables(Z * Y * own // GRID_W, head_size, K))
+    rows, width = gate_weight.shape
+    padded = -(-(width // 2) // 128) * 128
     D = residual.shape[1]
-    T, H, K = own, own // 2, kv.shape[1]
+    T, H = own, own // 2
     HH, DX = H // 2, D // X
     vmem = pl.BlockSpec(memory_space=pltpu.VMEM)
     hbm = pl.BlockSpec(memory_space=pl.ANY)
     return pl.pallas_call(
         kernel,
         out_shape=jax.ShapeDtypeStruct((own, D), bf16),
-        in_specs=[vmem, vmem, vmem, hbm, hbm, vmem],
+        in_specs=[hbm] * 12,
         out_specs=vmem,
         scratch_shapes=[
+            pltpu.VMEM(queries.shape, bf16),
+            pltpu.VMEM(keys.shape[::-1], bf16),
+            pltpu.VMEM(values.shape[::-1], bf16),
+            pltpu.VMEM(query_gain.shape, f32),
+            pltpu.VMEM(key_gain.shape, f32),
+            pltpu.VMEM((3, rows, width), bf16),
+            pltpu.VMEM(tables.shape, f32),
+            pltpu.VMEM((1, D), f32),
+            pltpu.VMEM((T, K), bf16),
+            pltpu.VMEM((T, K), bf16),
+            pltpu.VMEM((2, 3, rows, padded), bf16),
             pltpu.VMEM((Z, T, K), bf16),
             pltpu.VMEM((Y, T, K), bf16),
             pltpu.VMEM((3, D, padded), bf16),
             pltpu.VMEM((8 * K, D), bf16),
             pltpu.VMEM((Y * H, D), bf16),
-            pltpu.VMEM((2, Y, T, K), f32),
-            pltpu.VMEM((2, Y, T, K), f32),
+            pltpu.VMEM((2, Y * T, K), f32),
+            pltpu.VMEM((2, Y * T, K), f32),
             pltpu.VMEM((Y, 2, T, K), bf16),
             pltpu.VMEM((3, 2, T, K), bf16),
             pltpu.VMEM((T, K), bf16),
@@ -522,7 +612,10 @@
         compiler_params=pltpu.CompilerParams(
             collective_id=0, has_side_effects=True, vmem_limit_bytes=60 * 1024 * 1024
         ),
-    )(q, kv, pieces, out_weight, residual, norm_gain.reshape(1, D))
+    )(
+        queries, keys.T, values.T, query_gain, key_gain, gate_weight, up_weight, down_weight.T,
+        tables, out_weight, residual, norm_gain.reshape(1, D),
+    )
 
 
 def solution(mesh):

time: 135 us -> 107 us (0.79)
  Pallas kernels: 123 us -> 105 us
  local copies, waits for them, and re-layouts: 9.34 us -> 2.09 us
  other arithmetic: 2.12 us -> 0 us
    pallas_call x1, Pallas kernels: 123 us -> 105 us  [body(): pl.pallas_call(kernel, out_shape=jax.ShapeDtypeStruct((own, D), bf16), in...]
    unnamed x18 -> x1, local copies, waits for them, and re-layouts: 7.47 us -> 2.09 us
where the time goes in v2:
time: 107 us
  Pallas kernels  105 us (98%)
  local copies, waits for them, and re-layouts  2.09 us (2%)
    pallas_call x1, Pallas kernels, body(): pl.pallas_call(kernel, out_shape=jax.ShapeDtypeStruct((own, D), bf16), in...  105 us

profile of v2, /device:TPU:1, one launch (start us, length us, event | category | flops | bytes accessed | tf_op | source)
XLA Modules:
  0.0 106.8 jit_solution(257366603389932135)
XLA Ops:
  0.0 104.7 %shard_map.118 = bf16[192,2048]{1,0:T(8,128)(2,1)} custom-call(bf16[192,128]{1,0:T(8,128)(2,1)} %q_in.1, bf16[64,192]{1,0:T(8,128)(2,1)} %bitcast.5, bf16[64,192]{1,0:T(8,128)(2,1)} %bitcast.6, f32[2,64]{1,0:T(2,128)} %qg_in.1, f32[1,64]{1,0:T(1,128)} %kg_in.1, bf16[32,704]{1,0:T(8,128)(2,1)} %gate_in.1, bf16[32,704]{1,0:T(8,128)(2,1)} %up_in.1, ...), custom_call_target="tpu_custom_call" | custom-call | tf_op jit(solution)/shard_map/pallas_call | solution.py:572
  104.7 2.1 %copy.14 = bf16[192,2048]{1,0:T(8,128)(2,1)} copy(bf16[192,2048]{1,0:T(8,128)(2,1)} %shard_map.118) | data formatting | bytes 1572864

commit v3 on v2

--- a/solution.py
+++ b/solution.py
@@ -38,25 +38,28 @@
         return at
 
 
+COPIES = (
+    ("kvR", 16), ("kvL", 14), ("wR", 24), ("wL", 21), ("wD", 1), ("wE", 1), ("q", 1),
+    ("res", 3), ("resx", 3), ("owx", 3), ("owd", 1), ("comb", 1), ("comt", 1), ("att", 1),
+    ("ra1", 4), ("rb1", 4), ("ra2", 1), ("rb2", 1), ("outx", 6), ("outd", 1),
+)
+
+
 def plan():
     new = Sems()
-    names = {}
-    for name, count in (
-        ("kvR", 8), ("kvL", 7), ("wR", 24), ("wL", 21), ("wD", 16), ("wE", 16), ("wy", 2), ("q", 3),
-        ("res", 3), ("owx", 3), ("owd", 4), ("comb", 3), ("att", 32),
-        ("ra1", 12), ("rb1", 3), ("ra2", 3), ("rb2", 3), ("outx", 3), ("outd", 4),
-    ):
-        names[name] = (new(count), new(count))
+    names = {name: (new(1), new(count)) for name, count in COPIES}
+    names["wy"] = (new(2), new(2))
     names["local"] = (new(2), 0)
     names["in"] = (new(10), 0)
     return names, new.n
 
 
 SEMS, NSEMS = plan()
-W_AT = (2, 2, 1, 2)
-W_COMB = 3
+W_AT = (2, 2, 2, 2)
+W_COMB = 4
 W_ATT = 9
 W_GATE = 0
+LAG = 0
 
 
 def kernel(
@@ -64,7 +67,7 @@
     ow_ref, res_ref, ng_in, out_ref,
     q_raw, k_raw, v_raw, qg_raw, kg_raw, w_raw, tab, ng_ref,
     q_ref, kv_ref, wp_ref,
-    kvb, qb, wb, owb, resb, oacc, macc, cs, cr, ao, att, mid, nrm, hid, part,
+    kvb, qb, wb, owb, resb, oacc, macc, cs, cst, cr, crt, ao, att, mid, nrm, hid, part,
     rsa, rsb, a2, b2, rsa2, rsb2, sems,
 ):
     T = q_ref.shape[0]
@@ -90,18 +93,15 @@
 
     def remote(src, dst, name, i, to):
         return pltpu.make_async_remote_copy(
-            src_ref=src, dst_ref=dst, send_sem=ss(name, i), recv_sem=rs(name, i),
+            src_ref=src, dst_ref=dst, send_sem=ss(name), recv_sem=rs(name, i),
             device_id=to, device_id_type=MESH,
         )
 
     def got(dst, name, i=0):
         pltpu.make_async_copy(dst, dst, rs(name, i)).wait()
 
-    sent = []
-
     def go(copy):
         copy.start()
-        sent.append(copy)
 
     ins = [
         pltpu.make_async_copy(src, dst, ss("in", i))
@@ -173,16 +173,29 @@
     def slot(k):
         return lax.rem(z + k + Z, Z)
 
-    def kv_send(i):
-        left, right = kvb.at[slot(2 * i)], kvb.at[slot(-2 * i)]
-        srcL, srcR = (kv_ref, kv_ref) if i == 0 else (left, right)
-        go(remote(srcR, right, "kvR", 2 * i + 1, dev(zr2, y, x, c)))
-        if i < 3:
-            go(remote(srcL, left, "kvL", 2 * i + 1, dev(zl2, y, x, c)))
-        go(remote(srcR, right, "kvR", 2 * i, dev(zr, y, x, c)))
-        go(remote(srcL, left, "kvL", 2 * i, dev(zl, y, x, c)))
-
-    kv_send(0)
+    def kv_part(k, part_id):
+        return kvb.at[slot(k), pl.ds(part_id * H, H), :]
+
+    def kv_far(i, part_id):
+        for sign, name, to in ((-1, "kvR", zr2), (1, "kvL", zl2)):
+            if sign < 0 or i < 3:
+                block = kv_part(sign * 2 * i, part_id)
+                src = kv_ref.at[pl.ds(part_id * H, H), :] if i == 0 else block
+                go(remote(src, block, name, 2 * (2 * i + 1) + part_id, dev(to, y, x, c)))
+
+    def kv_near(i, part_id):
+        for sign, name, to in ((-1, "kvR", zr), (1, "kvL", zl)):
+            block = kv_part(sign * 2 * i, part_id)
+            src = kv_ref.at[pl.ds(part_id * H, H), :] if i == 0 else block
+            go(remote(src, block, name, 2 * (2 * i) + part_id, dev(to, y, x, c)))
+
+    def kv_got(k, part_id):
+        got(kv_part(k, part_id), "kvL" if k > 0 else "kvR", 2 * (abs(k) - 1) + part_id)
+
+    for part_id in (0, 1):
+        kv_far(0, part_id)
+    for part_id in (0, 1):
+        kv_near(0, part_id)
     for copy in ins[4:6]:
         copy.wait()
     query_gain = jnp.concatenate([qg_raw[0:1, :], qg_raw[1:2, :]], axis=1)
@@ -191,7 +204,7 @@
     qb[y] = q_ref[...]
     for k in (1, 2, 3):
         yk = lax.rem(y + k, Y)
-        go(remote(q_ref, qb.at[y], "q", k - 1, dev(z, yk, x, c)))
+        go(remote(q_ref, qb.at[y], "q", 0, dev(z, yk, x, c)))
     for copy in ins[6:]:
         copy.wait()
     units, padded = w_raw.shape[2] // 2, wp_ref.shape[3]
@@ -228,7 +241,7 @@
     for k in (1, 2, 3):
         xk = lax.rem(x + k, X)
         go(remote(ow_ref, owb.at[owrow, :], "owx", k - 1, dev(z, y, xk, c)))
-    go(remote(ow_ref, owb.at[owrow, :], "owd", 3, dev(z, y, x, o)))
+    go(remote(ow_ref, owb.at[owrow, :], "owd", 0, dev(z, y, x, o)))
     own_ow = pltpu.make_async_copy(ow_ref, owb.at[owrow, :], ss("local", 0))
     own_ow.start()
     half = pl.ds(pl.multiple_of(c * H, 32), H)
@@ -236,10 +249,25 @@
     own_res = pltpu.make_async_copy(res_ref.at[half, :], resb.at[own_rows, :], ss("local", 1))
     own_res.start()
 
+    y_cols = pl.ds(pl.multiple_of((x % 2) * DX, DX), 3 * DX)
+    pass_cols = pl.ds(pl.multiple_of((x % 2) * 3 * DX, DX), DX)
+    last_cols = pl.ds(pl.multiple_of((1 - x % 2) * 3 * DX, DX), DX)
+    x_pair = x + 1 - 2 * (x % 2)
+
+    def res_rows(k):
+        return pl.ds(pl.multiple_of(lax.rem(y + Y - k, Y) * H, 32), H)
+
     def res_send():
         for k in (1, 2, 3):
             yk = lax.rem(y + k, Y)
-            go(remote(res_ref.at[half, :], resb.at[own_rows, :], "res", k - 1, dev(z, yk, x, c)))
+            src, dst = res_ref.at[half, y_cols], resb.at[own_rows, y_cols]
+            go(remote(src, dst, "res", k - 1, dev(z, yk, x, c)))
+
+    def res_pass():
+        for k in (1, 3, 2):
+            got(resb.at[res_rows(k), y_cols], "res", k - 1)
+            block = resb.at[res_rows(k), pass_cols]
+            go(remote(block, block, "resx", k - 1, dev(z, y, x_pair, c)))
 
     res_send()
 
@@ -274,9 +302,9 @@
                 if i > 8 and not 0 < s < 8 or i == 8 and s == 0:
                     continue
                 share = w_shared(k, c, m)
-                go(remote(share, share, "wD" if m == 1 else "wE", i, dev(z, y, x, o)))
-
-    order = [(s + 2 * (m == 2), m, s) for s in range(9) for m in range(3)]
+                go(remote(share, share, "wD" if m == 1 else "wE", 0, dev(z, y, x, o)))
+
+    order = [(s + LAG * (m == 2), m, s) for s in range(9) for m in range(3)]
     todo_units = [(s, m) for _, m, s in sorted(order)]
 
     def w_units(count):
@@ -288,7 +316,7 @@
         xk = lax.rem(x + X - k, X)
         row = pl.ds(pl.multiple_of((xk * 2 + c) * 128, 128), 128)
         got(owb.at[row, :], "owx", k - 1)
-        go(remote(owb.at[row, :], owb.at[row, :], "owd", k - 1, dev(z, y, x, o)))
+        go(remote(owb.at[row, :], owb.at[row, :], "owd", 0, dev(z, y, x, o)))
 
     def attend(blocks, first):
         k0, k1, v0, v1 = [], [], [], []
@@ -329,50 +357,52 @@
             macc[h, rows] = top
 
     RB = 2 * T
+    got(qb.at[pl.ds(0, 3)], "q")
+    attend([kv_ref], True)
     for i in range(4):
         near, far = 2 * i + 1, 2 * i + 2
-        got(kvb.at[slot(-far)], "kvR", far - 1)
+        for part_id in (0, 1):
+            kv_got(-far, part_id)
+            if i < 3:
+                kv_got(far, part_id)
+                kv_far(i + 1, part_id)
         if i < 3:
-            got(kvb.at[slot(far)], "kvL", far - 1)
-            kv_send(i + 1)
-        got(kvb.at[slot(-near)], "kvR", near - 1)
-        got(kvb.at[slot(near)], "kvL", near - 1)
-        if i == 0:
-            for k in (1, 2, 3):
-                got(qb.at[lax.rem(y + Y - k, Y)], "q", k - 1)
+            for part_id in (0, 1):
+                kv_near(i + 1, part_id)
+        for part_id in (0, 1):
+            kv_got(-near, part_id)
+            kv_got(near, part_id)
         blocks = [kvb.at[slot(k)] for k in ((-near, near, -far, far) if i < 3 else (-near, near, -far))]
-        if i == 0:
-            attend([kv_ref], True)
         attend(blocks, False)
         w_units(W_AT[i])
+        if i == 2:
+            res_pass()
 
     low = lanes((T, K)) < K // 2
-    even = (lanes((T, K)) // (K // 4)) % 2 == 0
     for j in range(Y):
         rows = pl.ds(j * T, T)
         o0, o1 = oacc[0, rows], oacc[1, rows]
         total = jnp.where(low, pltpu.roll(o0, K // 2, 1), pltpu.roll(o1, K // 2, 1))
         level = jnp.where(low, macc[0, rows], macc[1, rows]) + jnp.log(total)
-        high = level.astype(bf16)
-        rest = (level - high.astype(f32)).astype(bf16)
-        cs[j, 0] = (jnp.where(low, o0, o1) / total).astype(bf16)
-        cs[j, 1] = jnp.where(even, high.astype(f32), rest.astype(f32)).astype(bf16)
+        cs[j] = (jnp.where(low, o0, o1) / total).astype(bf16)
+        across = level.T
+        cst[j, 0:8] = across[0:8]
+        cst[j, 8:16] = across[S : S + 8]
     for k in (1, 2, 3):
         yk = lax.rem(y + k, Y)
-        go(remote(cs.at[yk], cr.at[k - 1], "comb", k - 1, dev(z, yk, x, c)))
+        go(remote(cst.at[yk], crt.at[k - 1], "comt", 0, dev(z, yk, x, c)))
+        go(remote(cs.at[yk], cr.at[k - 1], "comb", 0, dev(z, yk, x, c)))
     w_units(W_COMB)
-    for k in (1, 2, 3):
-        got(cr.at[k - 1], "comb", k - 1)
-
-    def level_of(packed):
-        wide = packed.astype(f32)
-        return wide + jnp.where(
-            even, pltpu.roll(wide, K - K // 4, 1), pltpu.roll(wide, K // 4, 1)
-        )
-
-    own = cs.at[y]
-    outs = [own[0].astype(f32)] + [cr[k, 0].astype(f32) for k in range(3)]
-    levels = [level_of(own[1])] + [level_of(cr[k, 1]) for k in range(3)]
+    got(crt, "comt")
+    got(cr, "comb")
+
+    def level_of(across):
+        return jnp.concatenate(
+            [jnp.broadcast_to(across[i : i + 1], (S, T)) for i in (0, 8)], axis=0
+        ).T
+
+    outs = [cs[y].astype(f32)] + [cr[k].astype(f32) for k in range(3)]
+    levels = [level_of(cst[y])] + [level_of(crt[k]) for k in range(3)]
     top = functools.reduce(jnp.maximum, levels)
     shares = [jnp.exp(v - top) for v in levels]
     total = sum(shares[1:], shares[0])
@@ -386,7 +416,7 @@
         oc = other % 2
         return remote(
             ao.at[pl.ds(pl.multiple_of(oc * H, 32), H), :], att.at[own_rows, my_cols],
-            "att", k, (z * Y + other // 8, other % 8),
+            "att", 0, (z * Y + other // 8, other % 8),
         )
 
     def att_send(k, _):
@@ -402,24 +432,11 @@
     own_ow.wait()
     own_res.wait()
     for k in (1, 2, 3):
-        xk = lax.rem(x + X - k, X)
-        got(owb.at[pl.ds(pl.multiple_of((xk * 2 + o) * 128, 128), 128), :], "owd", k - 1)
-        yk = lax.rem(y + Y - k, Y)
-        got(resb.at[pl.ds(pl.multiple_of(yk * H, 32), H), :], "res", k - 1)
-    got(owb.at[pl.ds(pl.multiple_of((x * 2 + o) * 128, 128), 128), :], "owd", 3)
-
-    def att_wait(k, _):
-        other = lax.rem(me32 + 32 - k, 32)
-        got(
-            att.at[
-                pl.ds(pl.multiple_of((other // 8) * H, 32), H),
-                pl.ds(pl.multiple_of((other % 8) * K, K), K),
-            ],
-            "att", k,
-        )
-        return 0
-
-    lax.fori_loop(1, 32, att_wait, 0)
+        got(resb.at[res_rows(k), last_cols], "resx", k - 1)
+    got(owb.at[pl.ds(0, 4 * 128), :], "owd")
+
+    att_bytes = oacc.at[:, pl.ds(0, 31 * H // 4), :]
+    got(att_bytes, "att")
 
     NB = 512
 
@@ -447,21 +464,19 @@
 
     w_units(W_GATE)
 
-    def shared_in(m, name):
-        for s in range(9):
-            got(w_shared(-s, o, m), name, s)
-            if 0 < s < 8:
-                got(w_shared(s, o, m), name, 8 + s)
-
+    shared = {
+        "wD": wb.at[pl.ds(0, 2), pl.ds(0, 16 * 2 * R), :],
+        "wE": wb.at[pl.ds(2, 1), pl.ds(0, 16 * 2 * R), :],
+    }
     while any(m < 2 for _, m in todo_units):
         w_units(1)
-    shared_in(1, "wD")
+    got(shared["wD"], "wD")
     gate = jnp.dot(nrm[...], wb[0], preferred_element_type=f32)
     up = jnp.dot(nrm[...], wb[1], preferred_element_type=f32)
     hid[...] = (gate / (1.0 + jnp.exp(-gate)) * up).astype(bf16)
 
     w_units(len(todo_units))
-    shared_in(2, "wE")
+    got(shared["wE"], "wE")
 
     xcols = pl.ds(pl.multiple_of(x * DX, DX), DX)
 
@@ -474,42 +489,50 @@
         value = nt(hid[...], wb[2, cols, :]).astype(bf16)
         for j in range(Y):
             part[j, :, cols] = value[j * H : (j + 1) * H]
-        if k < 4:
-            go(
-                remote(
-                    part.at[:, pl.ds(HH, HH), cols], rsb.at[k - 1], "rb1", k - 1,
-                    dev(z, y, xk, c),
-                )
-            )
         for i in (1, 2, 3):
             yk = lax.rem(y + i, Y)
             go(
                 remote(
                     part.at[yk, pl.ds(0, HH), cols], rsa.at[i - 1, :, cols],
-                    "ra1", 4 * (i - 1) + k - 1, dev(z, yk, x, c),
+                    "ra1", k - 1, dev(z, yk, x, c),
                 )
             )
-    for k in (1, 2, 3):
-        for i in range(4):
-            got(rsa.at[k - 1, :, cols_of(lax.rem(x + i + 1, X))], "ra1", 4 * (k - 1) + i)
-    a2[...] = (
-        part[y, :HH, :].astype(f32)
-        + rsa[0].astype(f32) + rsa[1].astype(f32) + rsa[2].astype(f32)
-    ).astype(bf16)
-    for k in (1, 2, 3):
-        xk = lax.rem(x + k, X)
-        go(remote(a2.at[:, cols_of(xk)], rsa2.at[k - 1], "ra2", k - 1, dev(z, y, xk, c)))
-    for k in (1, 2, 3):
-        got(rsb.at[k - 1], "rb1", k - 1)
-    b2[...] = (
-        part[:, HH:, xcols].astype(f32)
-        + rsb[0].astype(f32) + rsb[1].astype(f32) + rsb[2].astype(f32)
-    ).astype(bf16)
-    for k in (1, 2, 3):
-        yk = lax.rem(y + k, Y)
-        go(remote(b2.at[yk], rsb2.at[k - 1], "rb2", k - 1, dev(z, yk, x, c)))
-    for k in (1, 2, 3):
-        got(rsa2.at[k - 1], "ra2", k - 1)
+    for i in (1, 2, 3, 4):
+        yk = lax.rem(y + i, Y)
+        for k in (1, 2, 3):
+            xk = lax.rem(x + k, X)
+            go(
+                remote(
+                    part.at[yk, pl.ds(HH, HH), cols_of(xk)], rsb.at[k - 1, yk],
+                    "rb1", i - 1, dev(z, y, xk, c),
+                )
+            )
+
+    def sum_a(i):
+        xk = lax.rem(x + i, X)
+        cols = cols_of(xk)
+        got(rsa.at[:, :, cols], "ra1", i - 1)
+        a2[:, cols] = (
+            part[y, :HH, cols].astype(f32) + rsa[0, :, cols].astype(f32)
+            + rsa[1, :, cols].astype(f32) + rsa[2, :, cols].astype(f32)
+        ).astype(bf16)
+        if i < 4:
+            go(remote(a2.at[:, cols], rsa2.at[i - 1], "ra2", 0, dev(z, y, xk, c)))
+
+    def sum_b(i):
+        yk = lax.rem(y + i, Y)
+        got(rsb.at[:, yk], "rb1", i - 1)
+        b2[yk] = (
+            part[yk, HH:, xcols].astype(f32) + rsb[0, yk].astype(f32)
+            + rsb[1, yk].astype(f32) + rsb[2, yk].astype(f32)
+        ).astype(bf16)
+        if i < 4:
+            go(remote(b2.at[yk], rsb2.at[i - 1], "rb2", 0, dev(z, yk, x, c)))
+
+    for i in (1, 2, 3, 4):
+        sum_a(i)
+        sum_b(i)
+    got(rsa2, "ra2")
     top_rows = pl.ds(pl.multiple_of(c * H, 16), HH)
     low_rows = pl.ds(pl.multiple_of(c * H + HH, 16), HH)
     ffn = (
@@ -518,40 +541,59 @@
     )
     mid_top = mid[pl.ds(pl.multiple_of(y * H, 16), HH), xcols]
     out_ref[top_rows, xcols] = (mid_top.astype(f32) + ffn).astype(bf16)
-    for k in (1, 2, 3):
-        got(rsb2.at[k - 1], "rb2", k - 1)
+
+    def out_send(rows, part_id):
+        mine = out_ref.at[rows, xcols]
+        for k in (1, 2, 3):
+            xk = lax.rem(x + k, X)
+            go(remote(mine, mine, "outx", 3 * part_id + k - 1, dev(z, y, xk, c)))
+        go(remote(mine, mine, "outd", 0, dev(z, y, x, o)))
+
+    def out_pass(rows, part_id):
+        for k in (1, 3, 2):
+            piece = out_ref.at[rows, cols_of(lax.rem(x + X - k, X))]
+            got(piece, "outx", 3 * part_id + k - 1)
+            go(remote(piece, piece, "outd", 0, dev(z, y, x, o)))
+
+    out_send(top_rows, 0)
+    got(rsb2, "rb2")
     ffn = b2[y].astype(f32) + rsb2[0].astype(f32) + rsb2[1].astype(f32) + rsb2[2].astype(f32)
     mid_low = mid[pl.ds(pl.multiple_of(y * H + HH, 16), HH), xcols]
     out_ref[low_rows, xcols] = (mid_low.astype(f32) + ffn).astype(bf16)
-
-    mine = out_ref.at[half, xcols]
-    for k in (1, 2, 3):
-        xk = lax.rem(x + k, X)
-        go(remote(mine, mine, "outx", k - 1, dev(z, y, xk, c)))
-    go(remote(mine, mine, "outd", 3, dev(z, y, x, o)))
-    for k in (1, 2, 3):
-        piece = out_ref.at[half, cols_of(lax.rem(x + X - k, X))]
-        got(piece, "outx", k - 1)
-        go(remote(piece, piece, "outd", k - 1, dev(z, y, x, o)))
-    other_half = pl.ds(pl.multiple_of(o * H, 32), H)
-    for k in (1, 2, 3):
-        got(out_ref.at[other_half, cols_of(lax.rem(x + X - k, X))], "outd", k - 1)
-    got(out_ref.at[other_half, xcols], "outd", 3)
-
-    for copy in sent:
-        copy.wait_send()
+    out_send(low_rows, 1)
+    out_pass(top_rows, 0)
+    out_pass(low_rows, 1)
+    got(rsb.at[pl.ds(0, 2)], "outd")
+
+    def left(ref, name):
+        pltpu.make_async_copy(ref, ref, ss(name)).wait()
+
+    left(kvb.at[pl.ds(0, 8)], "kvR")
+    left(kvb.at[pl.ds(0, 7)], "kvL")
+    left(wb.at[0, pl.ds(0, 24 * 2 * R), :], "wR")
+    left(wb.at[0, pl.ds(0, 21 * 2 * R), :], "wL")
+    left(shared["wD"], "wD")
+    left(shared["wE"], "wE")
+    left(qb.at[pl.ds(0, 3)], "q")
+    left(resb.at[pl.ds(0, 3 * H), y_cols], "res")
+    left(resb.at[pl.ds(0, 3 * H), pass_cols], "resx")
+    left(owb.at[pl.ds(0, 3 * 128), :], "owx")
+    left(owb.at[pl.ds(0, 4 * 128), :], "owd")
+    left(cr, "comb")
+    left(crt, "comt")
+    left(att_bytes, "att")
+    left(rsa, "ra1")
+    left(rsb, "rb1")
+    left(rsa2, "ra2")
+    left(rsb2, "rb2")
+    left(rsb.at[pl.ds(0, 2), pl.ds(0, 3)], "outx")
+    left(rsb.at[pl.ds(0, 2)], "outd")
     for j in (0, 1):
         to = 2 * c + j
 
         @pl.when(jnp.logical_not(jnp.logical_and(to == y, c == yc)))
         def _():
             pltpu.make_async_copy(wp_ref.at[j], wp_ref.at[j], ss("wy", j)).wait()
-
-    def att_left(k, _):
-        att_copy(k).wait_send()
-        return 0
-
-    lax.fori_loop(1, 32, att_left, 0)
 
 
 def body(
@@ -571,7 +613,7 @@
     hbm = pl.BlockSpec(memory_space=pl.ANY)
     return pl.pallas_call(
         kernel,
-        out_shape=jax.ShapeDtypeStruct((own, D), bf16),
+        out_shape=pltpu.VMEM((own, D), bf16),
         in_specs=[hbm] * 12,
         out_specs=vmem,
         scratch_shapes=[
@@ -593,8 +635,10 @@
             pltpu.VMEM((Y * H, D), bf16),
             pltpu.VMEM((2, Y * T, K), f32),
             pltpu.VMEM((2, Y * T, K), f32),
-            pltpu.VMEM((Y, 2, T, K), bf16),
-            pltpu.VMEM((3, 2, T, K), bf16),
+            pltpu.VMEM((Y, T, K), bf16),
+            pltpu.VMEM((Y, 16, T), f32),
+            pltpu.VMEM((3, T, K), bf16),
+            pltpu.VMEM((3, 16, T), f32),
             pltpu.VMEM((T, K), bf16),
             pltpu.VMEM((Y * H, 8 * K), bf16),
             pltpu.VMEM((Y * H, D), bf16),

time: 107 us -> 90.9 us (0.85)
  Pallas kernels: 105 us -> 89.8 us
  local copies, waits for them, and re-layouts: 2.09 us -> 0.88 us
    pallas_call x1, Pallas kernels: 105 us -> 89.8 us  [body(): pl.pallas_call(kernel, out_shape=pltpu.VMEM((own, D), bf16), in_specs=[hb...]
    unnamed x1, local copies, waits for them, and re-layouts: 2.09 us -> 0.88 us
where the time goes in v3:
time: 90.9 us; the launch traced here: 90.7 us
  Pallas kernels  89.8 us (99%)
    pallas_call x1, Pallas kernels, body(): pl.pallas_call(kernel, out_shape=pltpu.VMEM((own, D), bf16), in_specs=[hb...  89.8 us

profile of v3, /device:TPU:1, one launch (start us, length us, event | category | flops | bytes accessed | tf_op | source)
XLA Modules:
  0.0 90.7 jit_solution(4517649861458094412)
XLA Ops:
  0.0 89.8 %shard_map.118 = bf16[192,2048]{1,0:T(8,128)(2,1)S(1)} custom-call(bf16[192,128]{1,0:T(8,128)(2,1)} %q_in.1, bf16[64,192]{1,0:T(8,128)(2,1)} %bitcast.5, bf16[64,192]{1,0:T(8,128)(2,1)} %bitcast.6, f32[2,64]{1,0:T(2,128)} %qg_in.1, f32[1,64]{1,0:T(1,128)} %kg_in.1, bf16[32,704]{1,0:T(8,128)(2,1)} %gate_in.1, bf16[32,704]{1,0:T(8,128)(2,1)} %up_in.1, ...), custom_call_target="tpu_custom_call" | custom-call | tf_op jit(solution)/shard_map/pallas_call | solution.py:614
  89.8 0.9 copy.14

commit v4 on v3

--- a/solution.py
+++ b/solution.py
@@ -39,7 +39,7 @@
 
 
 COPIES = (
-    ("kvR", 16), ("kvL", 14), ("wR", 24), ("wL", 21), ("wD", 1), ("wE", 1), ("q", 1),
+    ("kvR", 16), ("kvL", 16), ("wR", 24), ("wL", 24), ("wD", 1), ("wE", 1), ("q", 1),
     ("res", 3), ("resx", 3), ("owx", 3), ("owd", 1), ("comb", 1), ("comt", 1), ("att", 1),
     ("ra1", 4), ("rb1", 4), ("ra2", 1), ("rb2", 1), ("outx", 6), ("outd", 1),
 )
@@ -55,7 +55,8 @@
 
 
 SEMS, NSEMS = plan()
-W_AT = (2, 2, 2, 2)
+W_FIRST = 0
+W_AT = (3, 2, 2, 2)
 W_COMB = 4
 W_ATT = 9
 W_GATE = 0
@@ -178,7 +179,7 @@
 
     def kv_far(i, part_id):
         for sign, name, to in ((-1, "kvR", zr2), (1, "kvL", zl2)):
-            if sign < 0 or i < 3:
+            if i < 3 or part_id == (sign > 0):
                 block = kv_part(sign * 2 * i, part_id)
                 src = kv_ref.at[pl.ds(part_id * H, H), :] if i == 0 else block
                 go(remote(src, block, name, 2 * (2 * i + 1) + part_id, dev(to, y, x, c)))
@@ -269,11 +270,11 @@
             block = resb.at[res_rows(k), pass_cols]
             go(remote(block, block, "resx", k - 1, dev(z, y, x_pair, c)))
 
-    res_send()
-
-    def wrows(k, core, m=None):
-        rows = pl.ds(pl.multiple_of((slot(k) * Y + 2 * core) * R, 2 * R), 2 * R)
-        return wb.at[:, rows, :] if m is None else wb.at[m, rows, :]
+    def w_block(sign, s, m, one=False):
+        one = one or s == 8
+        start = (slot(sign * s) * Y + 2 * c) * R + (R if one and sign > 0 else 0)
+        size = R if one else 2 * R
+        return wb.at[m, pl.ds(pl.multiple_of(start, R), size), :]
 
     def w_shared(k, core, m):
         rows = pl.ds(pl.multiple_of((slot(k) * Y + 2 * core) * R, 2 * R), 2 * R)
@@ -287,16 +288,13 @@
                 pltpu.make_async_copy(
                     wb.at[:, row, :], wb.at[:, row, :], sems.at[SEMS["wy"][1] + i]
                 ).wait()
-        if s > 0:
-            got(wrows(-s, c, m), "wR", 3 * (s - 1) + m)
-        if s < 8:
-            block = wrows(-s, c, m)
-            go(remote(block, block, "wR", 3 * s + m, dev(zr, y, x, c)))
-        if 0 < s < 8:
-            got(wrows(s, c, m), "wL", 3 * (s - 1) + m)
-        if s < 7:
-            block = wrows(s, c, m)
-            go(remote(block, block, "wL", 3 * s + m, dev(zl, y, x, c)))
+        for sign, name, to in ((-1, "wR", zr), (1, "wL", zl)):
+            if s > 0:
+                got(w_block(sign, s, m), name, 3 * (s - 1) + m)
+        for sign, name, to in ((-1, "wR", zr), (1, "wL", zl)):
+            if s < 8:
+                block = w_block(sign, s, m, s == 7)
+                go(remote(block, block, name, 3 * s + m, dev(to, y, x, c)))
         if m > 0:
             for i, k in ((s, -s), (8 + s, s)):
                 if i > 8 and not 0 < s < 8 or i == 8 and s == 0:
@@ -358,13 +356,17 @@
 
     RB = 2 * T
     got(qb.at[pl.ds(0, 3)], "q")
+    res_send()
     attend([kv_ref], True)
+    w_units(W_FIRST)
     for i in range(4):
         near, far = 2 * i + 1, 2 * i + 2
         for part_id in (0, 1):
-            kv_got(-far, part_id)
+            if i < 3 or part_id == 0:
+                kv_got(-far, part_id)
+            if i < 3 or part_id == 1:
+                kv_got(far, part_id)
             if i < 3:
-                kv_got(far, part_id)
                 kv_far(i + 1, part_id)
         if i < 3:
             for part_id in (0, 1):
@@ -568,10 +570,10 @@
     def left(ref, name):
         pltpu.make_async_copy(ref, ref, ss(name)).wait()
 
-    left(kvb.at[pl.ds(0, 8)], "kvR")
-    left(kvb.at[pl.ds(0, 7)], "kvL")
-    left(wb.at[0, pl.ds(0, 24 * 2 * R), :], "wR")
-    left(wb.at[0, pl.ds(0, 21 * 2 * R), :], "wL")
+    for name in ("kvR", "kvL"):
+        left(oacc.at[0, pl.ds(0, 15 * H // 2), :], name)
+    for name in ("wR", "wL"):
+        left(wb.at[0, pl.ds(0, 3 * 15 * R), :], name)
     left(shared["wD"], "wD")
     left(shared["wE"], "wE")
     left(qb.at[pl.ds(0, 3)], "q")

time: 90.9 us -> 90.1 us (level)
  no operation moved by 1% of the time
where the time goes in v4:
time: 90.1 us; the launch traced here: 90 us
  Pallas kernels  89.1 us (99%)
    pallas_call x1, Pallas kernels, body(): pl.pallas_call(kernel, out_shape=pltpu.VMEM((own, D), bf16), in_specs=[hb...  89.1 us

profile of v4, /device:TPU:1, one launch (start us, length us, event | category | flops | bytes accessed | tf_op | source)
XLA Modules:
  0.0 90.0 jit_solution(17362245572955378464)
XLA Ops:
  0.0 89.1 %shard_map.118 = bf16[192,2048]{1,0:T(8,128)(2,1)S(1)} custom-call(bf16[192,128]{1,0:T(8,128)(2,1)} %q_in.1, bf16[64,192]{1,0:T(8,128)(2,1)} %bitcast.5, bf16[64,192]{1,0:T(8,128)(2,1)} %bitcast.6, f32[2,64]{1,0:T(2,128)} %qg_in.1, f32[1,64]{1,0:T(1,128)} %kg_in.1, bf16[32,704]{1,0:T(8,128)(2,1)} %gate_in.1, bf16[32,704]{1,0:T(8,128)(2,1)} %up_in.1, ...), custom_call_target="tpu_custom_call" | custom-call | tf_op jit(solution)/shard_map/pallas_call | solution.py:616
  89.1 0.9 copy.14
